TPU v7x, 32 devices: a whole 2x2x4 slice. The times are simulated.
32 devices in a mesh: sp: 8 (over z, y), tp: 4 (over x, core).
Axes of the slice: x: 2, y: 2, z: 4, core: 2. Of those that a mesh axis runs over, the one named last changes fastest.
Arguments:
- stream: bfloat16 [1024, 2048], P('sp'), may hold values from -12 to 12
- out_grad: bfloat16 [1024, 2048], P('sp'), may hold values from -6 to 6
- routes: int32 [1024, 2], P('sp'), may hold values from 0 to 7, all different within a row; in each aligned block of 128 rows (0 to 127, 128 to 255, ...) at most 64 rows name the same one
- route_weight: float32 [1024, 2], P('sp'), may hold values from 0.2 to 1
- queries: bfloat16 [1024, 8, 128], P('sp', 'tp'), may hold values from -6 to 6
- key_vectors: bfloat16 [1024, 8, 128], P('sp', 'tp'), may hold values from -6 to 6
- value_vectors: bfloat16 [1024, 8, 256], P('sp', 'tp'), may hold values from -6 to 6
- log_decay: float32 [1024, 8], P('sp', 'tp'), may hold values from -1 to 0
- out_proj: bfloat16 [2048, 2048], P(None, 'tp'), may hold values from -0.125 to 0.125
- gate_weight: bfloat16 [8, 2048, 1024], P('sp', None, 'tp'), may hold values from -0.125 to 0.125
- up_weight: bfloat16 [8, 2048, 1024], P('sp', None, 'tp'), may hold values from -0.125 to 0.125
- down_weight: bfloat16 [8, 1024, 2048], P('sp', 'tp'), may hold values from -0.1875 to 0.1875
Outputs:
- gate_grad: bfloat16 [8, 2048, 1024], P('sp', None, 'tp')
- up_grad: bfloat16 [8, 2048, 1024], P('sp', None, 'tp')
- down_grad: bfloat16 [8, 1024, 2048], P('sp', 'tp')
- proj_grad: float32 [2048, 2048], P('sp', 'tp')
- query_grad: bfloat16 [1024, 8, 128], P('sp', 'tp')
- key_grad: bfloat16 [1024, 8, 128], P('sp', 'tp')
- value_grad: bfloat16 [1024, 8, 256], P('sp', 'tp')
Inputs may be any that keep to these rules, and one draw needn't show every extreme that they name: `routes`: each row names two different experts. In each aligned block of 128 rows no expert is named by more than 64 rows, and in some block an expert is named by exactly 64.
All inputs are finite; a program needn't handle non-finite values.
Results may differ from a plain program's by a relative error of at most 0.025.
Values may be sent and summed in bfloat16 or wider, within the bound.
A program may use at most 128 MiB of HBM per device.

v0:
```python
import functools

import jax
import jax.numpy as jnp
from jax import lax
from jax.experimental import pallas as pl
from jax.experimental.pallas import tpu as pltpu
from jax.sharding import PartitionSpec as P

CLAMP_LIMIT = 7.0
GATE_SLOPE = 1.702
EPSILON = 1e-06
F32 = jnp.float32
BF16 = jnp.bfloat16
MESH = pl.DeviceIdType.MESH


def any_specs(count):
    return [pl.BlockSpec(memory_space=pl.ANY)] * count


def vmem_specs(count):
    return [pl.BlockSpec(memory_space=pltpu.VMEM)] * count


def tp_partners(c, n_tp):
    far = lax.rem(c + n_tp // 2, n_tp)
    near = c + 1 - 2 * lax.rem(c, 2)
    return far, near


def greet(n_sp, me, c, sp_peers, tp_peers):
    barrier = pltpu.get_barrier_semaphore()
    count = 0
    if sp_peers:
        for k in range(1, n_sp):
            pl.semaphore_signal(
                barrier, inc=1, device_id=(lax.rem(me + k, n_sp), c), device_id_type=MESH
            )
            count += 1
    for t in tp_peers:
        pl.semaphore_signal(barrier, inc=1, device_id=(me, t), device_id_type=MESH)
        count += 1
    pl.semaphore_wait(barrier, count)


def push(src, dst, send_sem, recv_sem, device):
    return pltpu.make_async_remote_copy(
        src_ref=src,
        dst_ref=dst,
        send_sem=send_sem,
        recv_sem=recv_sem,
        device_id=device,
        device_id_type=MESH,
    )


class Chain:
    def __init__(self, src, out, n_sp, me, c, sems, ways):
        self.src, self.out, self.me, self.c = src, out, me, c
        self.pairs, self.ways = n_sp // 2, ways
        self.pair = me // 2
        self.other = me + 1 - 2 * lax.rem(me, 2)
        self.zs, self.zr, self.ys, self.yr, self.own_sem = sems

    def has(self, d, way):
        return self.pair >= d if way == 0 else self.pair + d < self.pairs

    def room(self, way):
        return self.pair + 1 < self.pairs if way == 0 else self.pair >= 1

    def spot(self, base, d, way):
        return self.out.at[base - 2 * d if way == 0 else base + 2 * d]

    def along(self, d, way):
        spot = self.spot(self.me, d, way)
        return push(
            self.src if d == 0 else spot, spot, self.zs.at[way, d], self.zr.at[way, d + 1],
            (self.me + 2 if way == 0 else self.me - 2, self.c),
        )

    def across(self, d, way):
        spot = self.spot(self.me, d, way)
        return push(
            self.src if d == 0 else spot, spot, self.ys.at[way, d], self.yr.at[way, d],
            (self.other, self.c),
        )

    def own(self):
        return pltpu.make_async_copy(self.src, self.out.at[self.me], self.own_sem.at[0])

    def each(self, d, act):
        for way in self.ways:

            @pl.when(self.has(d, way))
            def _():
                if d < self.pairs - 1:

                    @pl.when(self.room(way))
                    def _():
                        act(self.along(d, way))

                if d > 0 or way == self.ways[0]:
                    act(self.across(d, way))

    def start(self):
        self.own().start()
        self.each(0, lambda cp: cp.start())

    def step(self, d):
        for way in self.ways:

            @pl.when(self.has(d, way))
            def _():
                spot = self.spot(self.me, d, way)
                push(
                    spot, spot, self.zs.at[way, d], self.zr.at[way, d], (self.other, self.c)
                ).wait_recv()

        self.each(d, lambda cp: cp.start())

    def finish(self):
        for d in range(self.pairs):
            for way in self.ways:
                if d == 0 and way != self.ways[0]:
                    continue

                @pl.when(self.has(d, way))
                def _():
                    spot = self.spot(self.other, d, way)
                    push(
                        spot, spot, self.ys.at[way, d], self.yr.at[way, d], (self.other, self.c)
                    ).wait_recv()

            self.each(d, lambda cp: cp.wait_send())
        self.own().wait()


def chain_sems(n_sp):
    dma = pltpu.SemaphoreType.DMA
    return [dma((2, n_sp // 2))] * 4 + [dma((1,))]


def dispatch_kernel(
    n_sp, n_tp, q, rows, grads, tot, state, rows_out, grads_out, tot_out, states,
    own_sem, ssem, rsem, xssem, xrsem, dssem, drsem, essem, ersem, tssem, trsem, *chain_sem,
):
    me = lax.axis_index("sp")
    c = lax.axis_index("tp")
    far, near = tp_partners(c, n_tp)
    greet(n_sp, me, c, True, (far, near))
    arrays = ((rows, rows_out), (grads, grads_out))

    def cols(quarter):
        return pl.ds(pl.multiple_of(quarter * q, 128), q)

    chain = Chain(state, states, n_sp, me, c, chain_sem, (0,))
    chain.start()
    waits = []
    for k in range(1, n_sp):
        peer = lax.rem(me + k, n_sp)
        cp = push(tot, tot_out.at[me], tssem.at[k], trsem.at[k], (peer, c))
        cp.start()
        waits.append(cp)
        for a, (src, out) in enumerate(arrays):
            cp = push(
                src.at[peer], out.at[me, :, cols(c)], ssem.at[a, k], rsem.at[a, k], (peer, c)
            )
            cp.start()
            waits.append(cp)
    local = [pltpu.make_async_copy(tot, tot_out.at[me], own_sem.at[2])]
    for a, (src, out) in enumerate(arrays):
        local.append(pltpu.make_async_copy(src.at[me], out.at[me, :, cols(c)], own_sem.at[a]))
    for cp in local:
        cp.start()
    sent = []
    last = []

    def relay(k):
        source = lax.rem(me + n_sp - k, n_sp)
        for a, (src, out) in enumerate(arrays):
            spot = out.at[source, :, cols(far)]
            push(spot, spot, xssem.at[a, k], xrsem.at[a, k], (me, far)).wait_recv()
            cp = push(spot, spot, essem.at[a, k], ersem.at[a, k], (me, near))
            cp.start()
            sent.append(cp)
            last.append((out, source, a, k))

    for k in range(n_sp):
        source = lax.rem(me + n_sp - k, n_sp)
        for a, (src, out) in enumerate(arrays):
            spot = out.at[source, :, cols(c)]
            if k == 0:
                origin = src.at[me]
            else:
                push(spot, spot, ssem.at[a, k], rsem.at[a, k], (me, far)).wait_recv()
                origin = spot
            for sems, device in (((xssem, xrsem), far), ((dssem, drsem), near)):
                cp = push(origin, spot, sems[0].at[a, k], sems[1].at[a, k], (me, device))
                cp.start()
                sent.append(cp)
        if k >= 1:
            relay(k - 1)
        if k and k % 2 == 0:
            chain.step(k // 2)
    relay(n_sp - 1)
    near_far = lax.rem(near + n_tp // 2, n_tp)
    for out, source, a, k in last:
        spot = out.at[source, :, cols(near)]
        push(spot, spot, dssem.at[a, k], drsem.at[a, k], (me, near)).wait_recv()
        spot = out.at[source, :, cols(near_far)]
        push(spot, spot, essem.at[a, k], ersem.at[a, k], (me, near)).wait_recv()
    for k in range(1, n_sp):
        source = lax.rem(me + n_sp - k, n_sp)
        spot = tot_out.at[source]
        push(spot, spot, tssem.at[k], trsem.at[k], (me, far)).wait_recv()
    for cp in waits + sent:
        cp.wait_send()
    for cp in local:
        cp.wait()
    chain.finish()


def dispatch(rows, grads, tot, state, n_tp):
    n_sp, cap, q = rows.shape
    full = jax.ShapeDtypeStruct((n_sp, cap, q * n_tp), rows.dtype)
    dma = pltpu.SemaphoreType.DMA
    return pl.pallas_call(
        functools.partial(dispatch_kernel, n_sp, n_tp, q),
        out_shape=(
            full,
            full,
            jax.ShapeDtypeStruct((n_sp,) + tot.shape, tot.dtype),
            jax.ShapeDtypeStruct((n_sp,) + state.shape, state.dtype),
        ),
        in_specs=any_specs(4),
        out_specs=tuple(any_specs(4)),
        scratch_shapes=[dma((3,))] + [dma((2, n_sp))] * 8 + [dma((n_sp,))] * 2 + chain_sems(n_sp),
        compiler_params=pltpu.CompilerParams(collective_id=0, has_side_effects=True),
        name="dispatch",
    )(rows, grads, tot, state)


def return_kernel(
    n_sp, n_tp, q, back, comb, og, normed, resid, normed_all,
    part, xbuf, xrecv, sendbuf, ret, resq,
    pssem, prsem, xssem, xrsem, ssem, rsem, gssem, grsem, *chain_sem,
):
    me = lax.axis_index("sp")
    c = lax.axis_index("tp")
    far, near = tp_partners(c, n_tp)
    near_far = lax.rem(near + n_tp // 2, n_tp)
    greet(n_sp, me, c, True, (far, near))

    def cols(quarter):
        return pl.ds(pl.multiple_of(quarter * q, 128), q)

    order = list(range(1, n_sp)) + [0]
    waits = []
    for k in order:
        i = lax.rem(me + k, n_sp)
        for b, quarter in enumerate((near_far, near)):
            cp = push(
                back.at[i, :, cols(quarter)], part.at[b, k], pssem.at[b, k], prsem.at[b, k],
                (me, near),
            )
            cp.start()
            waits.append(cp)
    chain = Chain(normed, normed_all, n_sp, me, c, chain_sem, (0, 1))
    chain.start()

    def to_far(k):
        cp = push(xbuf.at[k], xrecv.at[k], xssem.at[k], xrsem.at[k], (me, far))
        cp.start()
        waits.append(cp)

    def to_home(k):
        cp = push(
            sendbuf.at[k], ret.at[me], ssem.at[k], rsem.at[k], (lax.rem(me + k, n_sp), c)
        )
        cp.start()
        waits.append(cp)

    def first(k):
        i = lax.rem(me + k, n_sp)
        push(xbuf.at[k], part.at[0, k], pssem.at[0, k], prsem.at[0, k], (me, near)).wait_recv()
        xbuf[k] = (back[i, :, cols(far)].astype(F32) + part[0, k].astype(F32)).astype(BF16)

    def second(k):
        i = lax.rem(me + k, n_sp)
        push(xbuf.at[k], part.at[1, k], pssem.at[1, k], prsem.at[1, k], (me, near)).wait_recv()
        push(xbuf.at[k], xrecv.at[k], xssem.at[k], xrsem.at[k], (me, far)).wait_recv()
        total = (
            back[i, :, cols(c)].astype(F32) + part[1, k].astype(F32) + xrecv[k].astype(F32)
        ).astype(BF16)
        if k == 0:
            ret[me] = total
        else:
            sendbuf[k] = total

    lag = 2
    for n in range(n_sp + lag + 1):
        if n < n_sp:
            first(order[n])
        if 1 <= n <= n_sp:
            to_far(order[n - 1])
        if lag <= n < n_sp + lag:
            second(order[n - lag])
        if n >= lag + 1 and order[n - lag - 1] != 0:
            to_home(order[n - lag - 1])
        if n and n % 3 == 0 and n // 3 < n_sp // 2:
            chain.step(n // 3)
    for d in range((n_sp + lag) // 3 + 1, n_sp // 2):
        chain.step(d)
    for k in range(1, n_sp):
        source = lax.rem(me + n_sp - k, n_sp)
        push(sendbuf.at[k], ret.at[source], ssem.at[k], rsem.at[k], (me, far)).wait_recv()
    cap = back.shape[1]
    returned = ret[...].astype(F32).reshape(n_sp * cap, q).astype(BF16)
    resq[...] = (
        og[...].astype(F32) + jnp.dot(comb[...], returned, preferred_element_type=F32)
    ).astype(BF16)
    mine = resid.at[:, cols(c)]
    own = pltpu.make_async_copy(resq, mine, gssem.at[3])
    own.start()
    for s, device in enumerate((far, near)):
        cp = push(resq, mine, gssem.at[s], grsem.at[s], (me, device))
        cp.start()
        waits.append(cp)
    spot = resid.at[:, cols(far)]
    push(resq, spot, gssem.at[0], grsem.at[0], (me, far)).wait_recv()
    cp = push(spot, spot, gssem.at[2], grsem.at[2], (me, near))
    cp.start()
    waits.append(cp)
    push(resq, resid.at[:, cols(near)], gssem.at[1], grsem.at[1], (me, near)).wait_recv()
    push(resq, resid.at[:, cols(near_far)], gssem.at[2], grsem.at[2], (me, near)).wait_recv()
    own.wait()
    for cp in waits:
        cp.wait_send()
    chain.finish()


def give_back(back, comb, og_q, normed, n_tp):
    n_sp, cap, width = back.shape
    q = width // n_tp
    tokens = og_q.shape[0]
    dma = pltpu.SemaphoreType.DMA
    block = pltpu.VMEM((n_sp, cap, q), BF16)
    return pl.pallas_call(
        functools.partial(return_kernel, n_sp, n_tp, q),
        out_shape=(
            jax.ShapeDtypeStruct((tokens, width), BF16),
            jax.ShapeDtypeStruct((n_sp,) + normed.shape, BF16),
        ),
        in_specs=vmem_specs(3) + any_specs(1),
        out_specs=tuple(any_specs(2)),
        scratch_shapes=[pltpu.VMEM((2, n_sp, cap, q), BF16)]
        + [block] * 4
        + [pltpu.VMEM((tokens, q), BF16)]
        + [dma((2, n_sp))] * 2
        + [dma((n_sp,))] * 4
        + [dma((4,)), dma((3,))]
        + chain_sems(n_sp),
        compiler_params=pltpu.CompilerParams(collective_id=1, has_side_effects=True),
        name="give_back",
    )(back, comb, og_q, normed)


def swap_kernel(n_sp, w, resid, state, cols_out, states, own_sem, ssem, rsem, *chain_sem):
    me = lax.axis_index("sp")
    c = lax.axis_index("tp")
    greet(n_sp, me, c, True, ())

    def part(index):
        if len(resid.shape) == 3:
            return resid.at[index]
        return resid.at[:, pl.ds(pl.multiple_of(index * w, 128), w)]

    chain = Chain(state, states, n_sp, me, c, chain_sem, (1,))
    chain.start()
    waits = []

    def send(k):
        peer = lax.rem(me + k, n_sp)
        cp = push(part(peer), cols_out.at[me], ssem.at[k], rsem.at[k], (peer, c))
        cp.start()
        waits.append(cp)

    local = pltpu.make_async_copy(part(me), cols_out.at[me], own_sem.at[0])
    local.start()
    for d in range(1, n_sp // 2):
        send(2 * d)
        send(2 * d - 1)
        chain.step(d)
    send(n_sp - 1)
    for k in range(1, n_sp):
        source = lax.rem(me + n_sp - k, n_sp)
        spot = cols_out.at[source]
        push(spot, spot, ssem.at[k], rsem.at[k], (source, c)).wait_recv()
    for cp in waits:
        cp.wait_send()
    local.wait()
    chain.finish()


def swap(resid, state, n_sp):
    tokens, width = resid.shape
    w = width // n_sp
    if w % 128:
        resid = resid.reshape(tokens, n_sp, w).transpose(1, 0, 2)
    dma = pltpu.SemaphoreType.DMA
    return pl.pallas_call(
        functools.partial(swap_kernel, n_sp, w),
        out_shape=(
            jax.ShapeDtypeStruct((n_sp, tokens, w), BF16),
            jax.ShapeDtypeStruct((n_sp,) + state.shape, BF16),
        ),
        in_specs=any_specs(2),
        out_specs=tuple(any_specs(2)),
        scratch_shapes=[dma((1,)), dma((n_sp,)), dma((n_sp,))] + chain_sems(n_sp),
        compiler_params=pltpu.CompilerParams(collective_id=2, has_side_effects=True),
        name="swap",
    )(resid, state)


def rotation_tables(start, count, key_width):
    frequency = 1.0 / 10000.0 ** jnp.linspace(0.0, 1.0, key_width // 2, dtype=F32)
    frequency = jnp.repeat(frequency, 2)
    token_position = (start + jnp.arange(count, dtype=jnp.int32)).astype(F32)
    angles = token_position[:, None] * frequency[None, :]
    return (jnp.cos(angles)[None], jnp.sin(angles)[None])


def swap_matrix(key_width):
    row = jnp.arange(key_width)[:, None]
    col = jnp.arange(key_width)[None, :]
    up = (col == row + 1) & (row % 2 == 0)
    down = (col == row - 1) & (row % 2 == 1)
    return (up.astype(F32) - down.astype(F32)).astype(BF16)


def turn(field, cosines, sines, matrix):
    turned = jnp.einsum("htk,kl->htl", field.astype(BF16), matrix, preferred_element_type=F32)
    return field.astype(F32) * cosines + turned * sines


def ein(spec, a, b):
    return jnp.einsum(spec, a.astype(BF16), b.astype(BF16), preferred_element_type=F32)


def fine(spec, a, b):
    return jnp.einsum(spec, a.astype(F32), b.astype(F32), precision=lax.Precision.HIGHEST)


def weighted(states, factors, present):
    kept = jnp.where(present[:, None, None, None], states.astype(F32), 0.0)
    return jnp.sum(kept * factors[:, :, None, None], axis=0)


def mm(a, b, da, db):
    return lax.dot_general(a, b, (((da,), (db,)), ((), ())), preferred_element_type=F32)


def expert_local(routed_rows, routed_grads, gate_w, up_w, down_w):
    gate_pre = mm(routed_rows, gate_w, 1, 0)
    up_pre = mm(routed_rows, up_w, 1, 0)
    gate_clip = jnp.minimum(gate_pre, CLAMP_LIMIT)
    up_clip = jnp.clip(up_pre, -CLAMP_LIMIT, CLAMP_LIMIT)
    sigmoid_gate = jax.nn.sigmoid(GATE_SLOPE * gate_clip)
    activated = (gate_clip * sigmoid_gate * (up_clip + 1.0)).astype(BF16)
    down_part = mm(activated, routed_grads, 0, 0)
    act_grad = mm(routed_grads, down_w, 1, 1)
    slope = sigmoid_gate + GATE_SLOPE * gate_clip * sigmoid_gate * (1.0 - sigmoid_gate)
    gate_pre_grad = jnp.where(
        gate_pre < CLAMP_LIMIT, act_grad * (up_clip + 1.0) * slope, 0.0
    ).astype(BF16)
    up_pre_grad = jnp.where(
        jnp.abs(up_pre) < CLAMP_LIMIT, act_grad * gate_clip * sigmoid_gate, 0.0
    ).astype(BF16)
    gate_part = mm(routed_rows, gate_pre_grad, 0, 0)
    up_part = mm(routed_rows, up_pre_grad, 0, 0)
    back_rows = mm(gate_pre_grad, gate_w, 1, 1) + mm(up_pre_grad, up_w, 1, 1)
    return (
        gate_part.astype(BF16),
        up_part.astype(BF16),
        down_part.astype(BF16),
        back_rows.astype(BF16),
    )


def per_device(
    stream, out_grad, routes, route_weight, queries, key_vectors, value_vectors, log_decay,
    out_proj, gate_weight, up_weight, down_weight,
):
    n_sp = lax.axis_size("sp")
    n_tp = lax.axis_size("tp")
    me = lax.axis_index("sp")
    tokens, width = stream.shape
    capacity = 4 * tokens // n_sp
    slots = n_sp * capacity
    quarter = width // n_tp
    heads = queries.shape[1]
    key_width = queries.shape[2]
    value_width = value_vectors.shape[2]

    ids = jnp.arange(n_sp, dtype=jnp.int32)
    chosen = routes[:, :, None] == ids[None, None, :]
    counts = jnp.sum(chosen.astype(F32), axis=1).astype(BF16)
    place = jnp.arange(tokens)
    lower = (place[:, None] > place[None, :]).astype(BF16)
    before = jnp.dot(lower, counts, preferred_element_type=F32)
    slot = jnp.sum(jnp.where(chosen, before[:, None, :], 0.0), axis=2).astype(jnp.int32)
    target = routes * capacity + slot
    spots = jnp.arange(slots, dtype=jnp.int32)
    hit = target.T[:, None, :] == spots[None, :, None]
    pick = (hit[0] | hit[1]).astype(BF16)
    weight = jnp.sum(
        jnp.where(hit[0], route_weight[None, :, 0], 0.0)
        + jnp.where(hit[1], route_weight[None, :, 1], 0.0),
        axis=1,
    )
    comb = ((target[:, :1] == spots[None, :]) | (target[:, 1:] == spots[None, :])).astype(BF16)
    col_start = lax.axis_index("tp") * quarter
    stream_q = lax.dynamic_slice_in_dim(stream, col_start, quarter, 1)
    og_q = lax.dynamic_slice_in_dim(out_grad, col_start, quarter, 1)
    send_rows = jnp.dot(pick, stream_q, preferred_element_type=F32).astype(BF16)
    send_grads = (
        weight[:, None] * jnp.dot(pick, og_q, preferred_element_type=F32)
    ).astype(BF16)

    running = jnp.cumsum(log_decay, axis=0).T
    block_total = running[:, -1]
    tot = jnp.broadcast_to(jnp.pad(block_total, (0, 128 - heads))[None, :], (8, 128))
    matrix = swap_matrix(key_width)
    cosines, sines = rotation_tables(me * tokens, tokens, key_width)
    scale = key_width ** (-0.5)
    query_rot = turn(queries.transpose(1, 0, 2), cosines, sines, matrix)
    key_rot = turn(key_vectors.transpose(1, 0, 2), cosines, sines, matrix) * scale
    values = value_vectors.transpose(1, 0, 2)
    causal = (place[:, None] >= place[None, :])[None]
    difference = running[:, :, None] - running[:, None, :]
    mask = jnp.where(causal, jnp.exp(jnp.where(causal, difference, 0.0)), 0.0)
    decay = jnp.exp(running)[..., None]
    remaining = jnp.exp(block_total[:, None] - running)[..., None]
    inner = ein("wfs,wfi->wsi", key_rot * remaining, values).astype(BF16)
    rows, grads, tots, inner_all = dispatch(
        send_rows.reshape(n_sp, capacity, quarter),
        send_grads.reshape(n_sp, capacity, quarter),
        tot,
        inner,
        n_tp,
    )
    key_bf = key_rot.astype(BF16)
    query_bf = query_rot.astype(BF16)
    weights = fine("hik,hjk->hij", query_rot, key_rot) * mask
    retained_local = fine("hij,hjv->hiv", weights, values)

    gate_part, up_part, down_part, back_rows = expert_local(
        rows.reshape(slots, width),
        grads.reshape(slots, width),
        gate_weight[0],
        up_weight[0],
        down_weight[0],
    )
    totals = tots[:, 0, :heads]
    sums = jnp.cumsum(totals, axis=0)
    sum_before = jnp.sum(jnp.where((ids < me)[:, None], totals, 0.0), axis=0)
    sum_through = sum_before + block_total
    past = jnp.where((ids < me)[:, None], sum_before[None] - sums, 0.0)
    past = jnp.where((ids < me)[:, None], jnp.exp(past), 0.0)
    coming = jnp.where((ids > me)[:, None], sums - totals - sum_through[None], 0.0)
    coming = jnp.where((ids > me)[:, None], jnp.exp(coming), 0.0)
    incoming = weighted(inner_all, past, ids < me)
    retained = retained_local + decay * fine("dzr,drs->dzs", query_rot, incoming)
    inverse_rms = lax.rsqrt(jnp.mean(retained * retained, axis=-1, keepdims=True) + EPSILON)
    normed = retained * inverse_rms
    normed_bf = normed.transpose(1, 0, 2).reshape(tokens, heads * value_width).astype(BF16)

    resid, normed_all = give_back(
        back_rows.reshape(n_sp, capacity, width), comb, og_q, normed_bf, n_tp
    )
    normed_grad = jnp.dot(resid, out_proj, preferred_element_type=F32)
    normed_grad = normed_grad.reshape(tokens, heads, value_width).transpose(1, 0, 2)
    grad = inverse_rms * (
        normed_grad - normed * jnp.mean(normed_grad * normed, axis=-1, keepdims=True)
    )
    grad_bf = grad.astype(BF16)
    inner_grad = ein("gwn,gwj->gnj", query_rot * decay, grad_bf).astype(BF16)
    resid_cols, grads_all = swap(resid, inner_grad, n_sp)
    future = weighted(grads_all, coming, ids > me).astype(BF16)
    score = fine("hiv,hjv->hij", grad, values) * mask
    query_portion = ein("hij,hjk->hik", score, key_bf) + decay * fine(
        "bpl,btl->bpt", grad, incoming
    )
    key_portion = ein("hij,hik->hjk", score, query_bf) + remaining * ein(
        "uxn,ubn->uxb", values, future
    )
    value_portion = ein("hij,hiv->hjv", weights, grad_bf) + remaining * ein(
        "bui,bim->bum", key_bf, future
    )
    query_grad = turn(query_portion, cosines, -sines, matrix).astype(BF16).transpose(1, 0, 2)
    key_grad = (
        (turn(key_portion, cosines, -sines, matrix) * scale).astype(BF16).transpose(1, 0, 2)
    )
    value_grad = value_portion.astype(BF16).transpose(1, 0, 2)
    proj_grad = mm(
        resid_cols.reshape(n_sp * tokens, -1), normed_all.reshape(n_sp * tokens, -1), 0, 0
    )
    return (
        gate_part[None],
        up_part[None],
        down_part[None],
        proj_grad,
        query_grad,
        key_grad,
        value_grad,
    )


def solution(mesh):
    in_specs = (
        P("sp", None),
        P("sp", None),
        P("sp", None),
        P("sp", None),
        P("sp", "tp", None),
        P("sp", "tp", None),
        P("sp", "tp", None),
        P("sp", "tp"),
        P(None, "tp"),
        P("sp", None, "tp"),
        P("sp", None, "tp"),
        P("sp", "tp", None),
    )
    out_specs = (
        P("sp", None, "tp"),
        P("sp", None, "tp"),
        P("sp", "tp", None),
        P("sp", "tp"),
        P("sp", "tp", None),
        P("sp", "tp", None),
        P("sp", "tp", None),
    )
    return jax.shard_map(
        per_device, mesh=mesh, in_specs=in_specs, out_specs=out_specs, check_vma=False
    )
```

profile of v0, /device:TPU:0, one launch (start us, length us, event | category | flops | bytes accessed | tf_op | source)
XLA Modules:
  0.0 165.9 jit_solution(13950932743710020655)
XLA Ops:
  0.8 0.8 slice_bitcast_fusion.5
  2.5 0.7 select_reduce_fusion
  4.1 1.0 copy.206
  5.1 1.0 copy.202
  6.1 0.8 copy.200
  9.3 0.8 fusion.38.comb
  10.4 0.9 constant_dynamic-slice_fusion.og
  12.5 0.8 convolution_convert_fusion.5.state
  13.7 1.1 fusion.3
  14.8 2.0 %convolution_convert_fusion.3 = bf16[512,512]{1,0:T(8,128)(2,1)} fusion(bf16[128,2048]{1,0:T(8,128)(2,1)} %param.12, s32[]{:T(128)S(6)} %select_n.92, pred[2,512,128]{2,1,0:T(32,128)(4,1)S(1)} %iota_compare_fusion), kind=kOutput, calls=%fused_computation.11 | convolution fusion | flops 67436544 | bytes 786436 | tf_op jit(solution)/shard_map/dot_general | solution.py:526
  16.8 40.5 %dispatch.1 = (bf16[8,64,2048]{2,1,0:T(8,128)(2,1)}, bf16[8,64,2048]{2,1,0:T(8,128)(2,1)}, f32[8,8,128]{2,1,0:T(8,128)}, bf16[8,2,128,256]{3,2,1,0:T(8,128)(2,1)}) custom-call(bf16[8,64,512]{2,1,0:T(8,128)(2,1)} %bitcast.195, bf16[8,64,512]{2,1,0:T(8,128)(2,1)} %bitcast.202, f32[8,128]{1,0:T(8,128)} %broadcast_in_dim.167.tot, ...), custom_call_target="tpu_custom_call" | custom-call | tf_op jit(solution)/shard_map/dispatch/pallas_call | solution.py:228
  57.3 0.8 slice.33
  59.3 1.6 multiply_reduce_fusion.1
  61.4 2.8 %fusion.20 = f32[512,256]{1,0:T(8,128)S(1)} fusion(bf16[512,2048]{1,0:T(8,128)(2,1)} %bitcast.208, bf16[1,2048,256]{2,1,0:T(8,128)(2,1)} %param.22), kind=kOutput, calls=%fused_computation.39 | convolution fusion | flops 536870912 | bytes 3670016 | tf_op jit(solution)/shard_map/dot_general | solution.py:461
  65.0 0.9 copy-done.24
  66.1 1.0 select_convert_fusion
  67.1 1.8 %fusion.2 = bf16[1,256,2048]{2,1,0:T(8,128)(2,1)} fusion(bf16[512,2048]{1,0:T(8,128)(2,1)S(1)} %bitcast.213, f32[512,256]{1,0:T(8,128)S(1)} %fusion.26, f32[512,256]{1,0:T(8,128)S(1)} %fusion.20), kind=kOutput, calls=%fused_computation.6 | convolution fusion | flops 538705920 | bytes 4194304 | tf_op jit(solution)/shard_map/dot_general | solution.py:461
  70.6 1.8 %fusion.1 = bf16[1,2048,256]{2,1,0:T(8,128)(2,1)} fusion(bf16[512,2048]{1,0:T(8,128)(2,1)S(1)} %bitcast.210, bf16[512,256]{1,0:T(8,128)(2,1)S(1)} %get-tuple-element.62), kind=kOutput, calls=%fused_computation.5 | convolution fusion | flops 537395200 | bytes 3407872 | tf_op jit(solution)/shard_map/dot_general | solution.py:461
  72.4 1.7 %fusion = bf16[1,2048,256]{2,1,0:T(8,128)(2,1)} fusion(bf16[512,2048]{1,0:T(8,128)(2,1)S(1)} %bitcast.211, bf16[512,256]{1,0:T(8,128)(2,1)S(1)} %get-tuple-element.63), kind=kOutput, calls=%fused_computation.4 | convolution fusion | flops 537395200 | bytes 3407872 | tf_op jit(solution)/shard_map/dot_general | solution.py:461
  74.1 0.7 fusion.24
  75.3 2.1 %add_convert_fusion = bf16[512,2048]{1,0:T(8,128)(2,1)} fusion(f32[512,2048]{1,0:T(8,128)S(1)} %fusion.24, bf16[512,256]{1,0:T(8,128)(2,1)S(1)} %get-tuple-element.62, bf16[1,2048,256]{2,1,0:T(8,128)(2,1)S(1)} %copy-done.4), kind=kOutput, calls=%fused_computation | convolution fusion | flops 538968064 | bytes 7602176 | tf_op jit(solution)/shard_map/dot_general | solution.py:461
  77.4 41.3 %give_back.1 = (bf16[128,2048]{1,0:T(8,128)(2,1)}, bf16[8,128,512]{2,1,0:T(8,128)(2,1)}) custom-call(bf16[8,64,2048]{2,1,0:T(8,128)(2,1)} %bitcast.194, bf16[128,512]{1,0:T(8,128)(2,1)} %fusion.38.comb, bf16[128,512]{1,0:T(8,128)(2,1)} %copy-done.5, bf16[128,512]{1,0:T(8,128)(2,1)} %bitcast.201), custom_call_target="tpu_custom_call" | custom-call | tf_op jit(solution)/shard_map/give_back/pallas_call | solution.py:349
  118.8 2.9 %fusion.93 = f32[128,512]{0,1:T(8,128)} fusion(bf16[128,2048]{1,0:T(8,128)(2,1)} %get-tuple-element.19.resid, bf16[2048,512]{1,0:T(8,128)(2,1)S(1)} %copy-done), kind=kOutput, calls=%fused_computation.166 | convolution fusion | flops 268435456 | bytes 2883584 | tf_op jit(solution)/shard_map/dot_general | solution.py:582
  121.7 1.1 copy.218
  122.7 0.9 fusion.28
  123.6 0.8 fusion.29
  124.8 1.0 fusion.18
  126.3 0.8 convolution_convert_fusion.4.state
  127.6 1.0 fusion.16
  129.3 31.3 %swap.1 = (bf16[8,128,256]{2,1,0:T(8,128)(2,1)}, bf16[8,2,128,256]{3,2,1,0:T(8,128)(2,1)}) custom-call(bf16[128,2048]{1,0:T(8,128)(2,1)} %get-tuple-element.19.resid, bf16[2,128,256]{2,1,0:T(8,128)(2,1)} %convolution_convert_fusion.4.state), custom_call_target="tpu_custom_call" | custom-call | tf_op jit(solution)/shard_map/swap/pallas_call | solution.py:412
  160.6 2.7 %convolution_bitcast_fusion = f32[256,512]{1,0:T(8,128)} fusion(bf16[8,128,256]{2,1,0:T(8,128)(2,1)} %get-tuple-element.20, bf16[8,128,512]{2,1,0:T(8,128)(2,1)} %get-tuple-element.21), kind=kOutput, calls=%fused_computation.12 | convolution fusion | flops 268435456 | bytes 2097152 | tf_op jit(solution)/shard_map/dot_general | solution.py:461
  165.1 0.8 copy.240
  (107 shorter events, 14.6 us)
Async XLA Ops:
  0.6 118.2 %copy-start = (bf16[2048,512]{1,0:T(8,128)(2,1)S(1)}, bf16[2048,512]{1,0:T(8,128)(2,1)}, u32[]{:S(2)}) copy-start(bf16[2048,512]{1,0:T(8,128)(2,1)} %param.20) | copy-start | bytes 6291460
  0.6 11.8 %copy-start.1 = (bf16[128,2,256]{2,1,0:T(2,128)(2,1)S(1)}, bf16[128,2,256]{2,1,0:T(2,128)(2,1)}, u32[]{:S(2)}) copy-start(bf16[128,2,256]{2,1,0:T(2,128)(2,1)} %param.18) | copy-start | bytes 393220
  0.8 57.7 %copy-start.21 = (pred[8]{0:T(512)(128)(4,1)}, pred[8]{0:T(512)(128)(4,1)S(1)}, u32[]{:S(2)}) copy-start(pred[8]{0:T(512)(128)(4,1)S(1)} %get-tuple-element.81) | copy-start | bytes 28
  1.6 13.2 %copy-start.12 = (pred[128]{0:T(512)(128)(4,1)}, pred[128]{0:T(512)(128)(4,1)S(1)}, u32[]{:S(2)}) copy-start(pred[128]{0:T(512)(128)(4,1)S(1)} %get-tuple-element.79) | copy-start | bytes 388
  1.6 13.2 %copy-start.14 = (pred[128]{0:T(512)(128)(4,1)}, pred[128]{0:T(512)(128)(4,1)S(1)}, u32[]{:S(2)}) copy-start(pred[128]{0:T(512)(128)(4,1)S(1)} %get-tuple-element.80) | copy-start | bytes 388
  1.6 13.2 %copy-start.16 = (s32[128]{0:T(128)}, s32[128]{0:T(128)S(1)}, u32[]{:S(2)}) copy-start(s32[128]{0:T(128)S(1)} %get-tuple-element.83) | copy-start | bytes 1540
  1.7 13.1 %copy-start.18 = (s32[128]{0:T(128)}, s32[128]{0:T(128)S(1)}, u32[]{:S(2)}) copy-start(s32[128]{0:T(128)S(1)} %get-tuple-element.84) | copy-start | bytes 1540
  7.1 9.7 %copy-start.6 = (f32[128,2]{0,1:T(2,128)}, f32[128,2]{0,1:T(2,128)S(1)}, u32[]{:S(2)}) copy-start(f32[128,2]{0,1:T(2,128)S(1)} %copy.201) | copy-start | bytes 3076
  8.0 60.9 %copy-start.8 = (f32[2,128]{1,0:T(2,128)}, f32[2,128]{1,0:T(2,128)S(1)}, u32[]{:S(2)}) copy-start(f32[2,128]{1,0:T(2,128)S(1)} %get-tuple-element.73) | copy-start | bytes 3076
  9.3 60.5 %copy-start.11 = (f32[128,2]{0,1:T(2,128)}, f32[128,2]{0,1:T(2,128)S(1)}, u32[]{:S(2)}) copy-start(f32[128,2]{0,1:T(2,128)S(1)} %copy.212) | copy-start | bytes 3076
  11.3 46.1 %copy-start.5 = (bf16[128,512]{1,0:T(8,128)(2,1)}, bf16[128,512]{1,0:T(8,128)(2,1)S(1)}, u32[]{:S(2)}) copy-start(bf16[128,512]{1,0:T(8,128)(2,1)S(1)} %constant_dynamic-slice_fusion.og) | copy-start | bytes 393220
  60.9 3.3 %copy-start.3 = (bf16[1,2048,256]{2,1,0:T(8,128)(2,1)S(1)}, bf16[1,2048,256]{2,1,0:T(8,128)(2,1)}, u32[]{:S(2)}) copy-start(bf16[1,2048,256]{2,1,0:T(8,128)(2,1)} %param.21) | copy-start | bytes 3145732
  60.9 3.3 %copy-start.23 = (bf16[8,64,2048]{2,1,0:T(8,128)(2,1)S(1)}, bf16[8,64,2048]{2,1,0:T(8,128)(2,1)}, u32[]{:S(2)}) copy-start(bf16[8,64,2048]{2,1,0:T(8,128)(2,1)} %get-tuple-element.15) | copy-start | bytes 6291460
  64.2 1.6 copy-start.24
  64.2 1.8 %copy-start.25 = (bf16[1,256,2048]{2,1,0:T(8,128)(2,1)S(1)}, bf16[1,256,2048]{2,1,0:T(8,128)(2,1)}, u32[]{:S(2)}) copy-start(bf16[1,256,2048]{2,1,0:T(8,128)(2,1)} %param.23) | copy-start | bytes 3145732
  74.1 1.2 copy-start.4
  122.7 3.5 %copy-start.9 = (f32[2,128]{1,0:T(2,128)S(1)}, f32[2,128]{1,0:T(2,128)}, u32[]{:S(2)}) copy-start(f32[2,128]{1,0:T(2,128)} %copy-done.8) | copy-start | bytes 3076
  127.3 35.9 %copy-start.7 = (f32[8,2]{1,0:T(8,128)S(1)}, f32[8,2]{1,0:T(8,128)}, u32[]{:S(2)}) copy-start(f32[8,2]{1,0:T(8,128)} %copy.231) | copy-start | bytes 196
  127.4 35.9 %copy-start.22 = (pred[8]{0:T(512)(128)(4,1)S(1)}, pred[8]{0:T(512)(128)(4,1)}, u32[]{:S(2)}) copy-start(pred[8]{0:T(512)(128)(4,1)} %copy-done.21) | copy-start | bytes 28
  128.5 35.1 %copy-start.10 = (f32[128,2]{0,1:T(2,128)S(1)}, f32[128,2]{0,1:T(2,128)}, u32[]{:S(2)}) copy-start(f32[128,2]{0,1:T(2,128)} %copy.230) | copy-start | bytes 3076
  160.5 2.8 %copy-start.2 = (bf16[8,2,128,256]{3,2,1,0:T(8,128)(2,1)S(1)}, bf16[8,2,128,256]{3,2,1,0:T(8,128)(2,1)}, u32[]{:S(2)}) copy-start(bf16[8,2,128,256]{3,2,1,0:T(8,128)(2,1)} %get-tuple-element.22) | copy-start | bytes 3145732
  160.5 3.6 %copy-start.13 = (pred[128]{0:T(512)(128)(4,1)S(1)}, pred[128]{0:T(512)(128)(4,1)}, u32[]{:S(2)}) copy-start(pred[128]{0:T(512)(128)(4,1)} %copy-done.12) | copy-start | bytes 388
  160.5 3.6 %copy-start.15 = (pred[128]{0:T(512)(128)(4,1)S(1)}, pred[128]{0:T(512)(128)(4,1)}, u32[]{:S(2)}) copy-start(pred[128]{0:T(512)(128)(4,1)} %copy-done.14) | copy-start | bytes 388
  160.6 3.6 %copy-start.17 = (s32[128]{0:T(128)S(1)}, s32[128]{0:T(128)}, u32[]{:S(2)}) copy-start(s32[128]{0:T(128)} %copy-done.16) | copy-start | bytes 1540
  160.6 3.6 %copy-start.19 = (s32[128]{0:T(128)S(1)}, s32[128]{0:T(128)}, u32[]{:S(2)}) copy-start(s32[128]{0:T(128)} %copy-done.18) | copy-start | bytes 1540
  160.6 3.6 %copy-start.20 = (f32[2,128]{1,0:T(2,128)S(1)}, f32[2,128]{1,0:T(2,128)}, u32[]{:S(2)}) copy-start(f32[2,128]{1,0:T(2,128)} %get-tuple-element.61) | copy-start | bytes 3076
where the time goes:
time: 167 us; the launch traced here: 166 us
  Pallas kernels  113 us (68%)
  matrix products  28.6 us (17%)
  local copies, waits for them, and re-layouts  13.9 us (8%)
  other arithmetic  9.13 us (5%)
    pallas_call x1, Pallas kernels, give_back(): pl.pallas_call(functools.partial(return_kernel, n_sp, n_tp, q), out_shape...  41.3 us
    pallas_call x1, Pallas kernels, dispatch(): pl.pallas_call(functools.partial(dispatch_kernel, n_sp, n_tp, q), out_sha...  40.5 us
    pallas_call x1, Pallas kernels, swap(): pl.pallas_call(functools.partial(swap_kernel, n_sp, w), out_shape=(jax.Sh...  31.3 us
    dot_general x9, matrix products, mm(): lax.dot_general(a, b, (((da,), (db,)), ((), ())), preferred_element_type=...  15.3 us
    unnamed x58, local copies, waits for them, and re-layouts  6.61 us

commit v1 on v0

v1 whole, which is shorter than its diff:
```python
import functools

import jax
import jax.numpy as jnp
from jax import lax
from jax.experimental import pallas as pl
from jax.experimental.pallas import tpu as pltpu
from jax.sharding import PartitionSpec as P

CLAMP_LIMIT = 7.0
GATE_SLOPE = 1.702
EPSILON = 1e-06
F32 = jnp.float32
BF16 = jnp.bfloat16
MESH = pl.DeviceIdType.MESH


def any_specs(count):
    return [pl.BlockSpec(memory_space=pl.ANY)] * count


def vmem_specs(count):
    return [pl.BlockSpec(memory_space=pltpu.VMEM)] * count


def tp_partners(c, n_tp):
    far = lax.rem(c + n_tp // 2, n_tp)
    near = c + 1 - 2 * lax.rem(c, 2)
    return far, near


def greet(n_sp, me, c, sp_peers, tp_peers):
    barrier = pltpu.get_barrier_semaphore()
    count = 0
    if sp_peers:
        for k in range(1, n_sp):
            pl.semaphore_signal(
                barrier, inc=1, device_id=(lax.rem(me + k, n_sp), c), device_id_type=MESH
            )
            count += 1
    for t in tp_peers:
        pl.semaphore_signal(barrier, inc=1, device_id=(me, t), device_id_type=MESH)
        count += 1
    pl.semaphore_wait(barrier, count)


def push(src, dst, send_sem, recv_sem, device):
    return pltpu.make_async_remote_copy(
        src_ref=src,
        dst_ref=dst,
        send_sem=send_sem,
        recv_sem=recv_sem,
        device_id=device,
        device_id_type=MESH,
    )


class Chain:
    def __init__(self, src, out, n_sp, me, c, sems, ways):
        self.src, self.out, self.me, self.c = src, out, me, c
        self.pairs, self.ways = n_sp // 2, ways
        self.pair = me // 2
        self.other = me + 1 - 2 * lax.rem(me, 2)
        self.zs, self.zr, self.ys, self.yr, self.own_sem = sems

    def has(self, d, way):
        return self.pair >= d if way == 0 else self.pair + d < self.pairs

    def room(self, way):
        return self.pair + 1 < self.pairs if way == 0 else self.pair >= 1

    def spot(self, base, d, way):
        return self.out.at[base - 2 * d if way == 0 else base + 2 * d]

    def along(self, d, way):
        spot = self.spot(self.me, d, way)
        return push(
            self.src if d == 0 else spot, spot, self.zs.at[way, d], self.zr.at[way, d + 1],
            (self.me + 2 if way == 0 else self.me - 2, self.c),
        )

    def across(self, d, way):
        spot = self.spot(self.me, d, way)
        return push(
            self.src if d == 0 else spot, spot, self.ys.at[way, d], self.yr.at[way, d],
            (self.other, self.c),
        )

    def own(self):
        return pltpu.make_async_copy(self.src, self.out.at[self.me], self.own_sem.at[0])

    def each(self, d, act):
        for way in self.ways:

            @pl.when(self.has(d, way))
            def _():
                if d < self.pairs - 1:

                    @pl.when(self.room(way))
                    def _():
                        act(self.along(d, way))

                if d > 0 or way == self.ways[0]:
                    act(self.across(d, way))

    def start(self):
        self.own().start()
        self.each(0, lambda cp: cp.start())

    def step(self, d):
        for way in self.ways:

            @pl.when(self.has(d, way))
            def _():
                spot = self.spot(self.me, d, way)
                push(
                    spot, spot, self.zs.at[way, d], self.zr.at[way, d], (self.other, self.c)
                ).wait_recv()

        self.each(d, lambda cp: cp.start())

    def finish(self):
        for d in range(self.pairs):
            for way in self.ways:
                if d == 0 and way != self.ways[0]:
                    continue

                @pl.when(self.has(d, way))
                def _():
                    spot = self.spot(self.other, d, way)
                    push(
                        spot, spot, self.ys.at[way, d], self.yr.at[way, d], (self.other, self.c)
                    ).wait_recv()

            self.each(d, lambda cp: cp.wait_send())
        self.own().wait()


def chain_sems(n_sp):
    dma = pltpu.SemaphoreType.DMA
    return [dma((2, n_sp // 2))] * 4 + [dma((1,))]


def dot(a, b, da, db):
    return lax.dot_general(a, b, (((da,), (db,)), ((), ())), preferred_element_type=F32)


def flat(block):
    n, cap, q = block.shape
    if cap % 16 == 0:
        return block.reshape(n * cap, q)
    return block.astype(F32).reshape(n * cap, q).astype(BF16)


def experts_kernel(
    n_sp, n_tp, pack, pick, og, gate_w, up_w, down_w, tot, state,
    gate_o, up_o, down_o, resid, tot_out, states,
    full, gu, dw, act, gug, back, part, xbuf, xrecv, sendbuf, ret, resq, gout, uout, dout,
    wsem, osem, own_sem, ssem, rsem, fs, fr, ns, nr, es, er, ps, pr, xs, xr, hs, hr,
    gs, gr, tssem, trsem, *chain_sem,
):
    me = lax.axis_index("sp")
    c = lax.axis_index("tp")
    far, near = tp_partners(c, n_tp)
    near_far = lax.rem(near + n_tp // 2, n_tp)
    cap, q = pack.shape[2:]
    hid = dw.shape[0]
    loads = [
        pltpu.make_async_copy(gate_w.at[0], gu.at[:, pl.ds(0, hid)], wsem.at[0]),
        pltpu.make_async_copy(up_w.at[0], gu.at[:, pl.ds(hid, hid)], wsem.at[1]),
        pltpu.make_async_copy(down_w.at[0], dw, wsem.at[2]),
    ]
    for cp in loads:
        cp.start()
    greet(n_sp, me, c, True, (far, near))

    def source(k):
        return lax.rem(me + n_sp - k, n_sp)

    def out_copy(k):
        peer = lax.rem(me + k, n_sp)
        return push(pack.at[peer], full.at[me, c], ssem.at[k], rsem.at[k], (peer, c))

    def tot_copy(k):
        peer = lax.rem(me + k, n_sp)
        return push(tot, tot_out.at[me], tssem.at[k], trsem.at[k], (peer, c))

    def far_copy(k, quarter, own=False):
        spot = full.at[source(k), quarter]
        return push(pack.at[me] if own else spot, spot, fs.at[k], fr.at[k], (me, far))

    def near_copy(k, quarter, own=False):
        spot = full.at[source(k), quarter]
        return push(pack.at[me] if own else spot, spot, ns.at[k], nr.at[k], (me, near))

    def relay_copy(k, quarter):
        spot = full.at[source(k), quarter]
        return push(spot, spot, es.at[k], er.at[k], (me, near))

    def part_copy(k, b):
        quarter = near_far if b == 0 else near
        return push(
            back.at[k, quarter], part.at[b, k], ps.at[b, k], pr.at[b, k], (me, near)
        )

    def x_copy(k):
        return push(xbuf.at[k], xrecv.at[k], xs.at[k], xr.at[k], (me, far))

    def home_copy(k):
        return push(sendbuf.at[k], ret.at[me], hs.at[k], hr.at[k], (source(k), c))

    far_copy(0, c, True).start()
    near_copy(0, c, True).start()
    for k in range(1, n_sp):
        out_copy(k).start()
    for k in range(1, n_sp):
        tot_copy(k).start()
    own_tot = pltpu.make_async_copy(tot, tot_out.at[me], own_sem.at[0])
    own_tot.start()
    chain = Chain(state, states, n_sp, me, c, chain_sem, (0,))
    chain.start()
    full[me, c] = pack[me]
    for cp in loads:
        cp.wait()

    def compute(k):
        src = source(k)
        near_copy(k, near).wait_recv()
        relay_copy(k, near_far).wait_recv()
        pre = None
        act_grad = None
        for t in range(n_tp):
            cols = pl.ds(t * q, q)
            a = dot(full[src, t, 0], gu[cols, :], 1, 0)
            b = dot(full[src, t, 1], dw[:, cols], 1, 1)
            pre = a if t == 0 else pre + a
            act_grad = b if t == 0 else act_grad + b
        gate_pre = pre[:, :hid]
        up_pre = pre[:, hid:]
        gate_clip = jnp.minimum(gate_pre, CLAMP_LIMIT)
        up_clip = jnp.clip(up_pre, -CLAMP_LIMIT, CLAMP_LIMIT)
        sig = 1.0 / (1.0 + jnp.exp(-GATE_SLOPE * gate_clip))
        gated = gate_clip * sig
        act[src] = (gated * (up_clip + 1.0)).astype(BF16)
        slope = sig + GATE_SLOPE * gated * (1.0 - sig)
        gpg = jnp.where(gate_pre < CLAMP_LIMIT, act_grad * (up_clip + 1.0) * slope, 0.0)
        upg = jnp.where(jnp.abs(up_pre) < CLAMP_LIMIT, act_grad * gated, 0.0)
        both = jnp.concatenate([gpg, upg], axis=1).astype(BF16)
        gug[src] = both
        for t in range(n_tp):
            back[k, t] = dot(both, gu[pl.ds(t * q, q), :], 1, 1).astype(BF16)

    def first(k):
        part_copy(k, 0).wait_recv()
        xbuf[k] = (back[k, far].astype(F32) + part[0, k].astype(F32)).astype(BF16)
        x_copy(k).start()

    def second(k):
        part_copy(k, 1).wait_recv()
        x_copy(k).wait_recv()
        total = (
            back[k, c].astype(F32) + part[1, k].astype(F32) + xrecv[k].astype(F32)
        ).astype(BF16)

        @pl.when(k == 0)
        def _():
            ret[me] = total

        @pl.when(k > 0)
        def _():
            sendbuf[k] = total
            home_copy(k).start()

    def relay_far(k):
        far_copy(k, far).wait_recv()
        relay_copy(k, far).start()

    def step(n, carry):
        @pl.when((n >= 1) & (n < n_sp))
        def _():
            out_copy(n).wait_recv()
            far_copy(n, c).start()
            near_copy(n, c).start()

        @pl.when((n >= 1) & (n <= n_sp))
        def _():
            relay_far(n - 1)

        for d in range(1, n_sp // 2):

            @pl.when(n == 2 * d)
            def _():
                chain.step(d)

        @pl.when((n >= 2) & (n < n_sp + 2))
        def _():
            compute(n - 2)
            part_copy(n - 2, 0).start()
            part_copy(n - 2, 1).start()

        @pl.when((n >= 3) & (n < n_sp + 3))
        def _():
            first(n - 3)

        @pl.when((n >= 4) & (n < n_sp + 4))
        def _():
            second(n - 4)

        return carry

    lax.fori_loop(0, n_sp + 4, step, 0)

    def weights_grad(t, carry):
        cols = pl.ds(pl.multiple_of(t * q, 128), q)
        x = flat(full[:, t, 0])
        g = flat(full[:, t, 1])
        both = dot(x, flat(gug[...]), 0, 0).astype(BF16)
        gout[cols, :] = both[:, :hid]
        uout[cols, :] = both[:, hid:]
        dout[:, cols] = dot(flat(act[...]), g, 0, 0).astype(BF16)
        return carry

    lax.fori_loop(0, n_tp, weights_grad, 0)
    stores = [
        pltpu.make_async_copy(gout, gate_o.at[0], osem.at[0]),
        pltpu.make_async_copy(uout, up_o.at[0], osem.at[1]),
        pltpu.make_async_copy(dout, down_o.at[0], osem.at[2]),
    ]
    for cp in stores:
        cp.start()

    def arrive(k, carry):
        home = lax.rem(me + k, n_sp)
        push(sendbuf.at[k], ret.at[home], hs.at[k], hr.at[k], (home, c)).wait_recv()
        return carry

    lax.fori_loop(1, n_sp, arrive, 0)
    resq[...] = (og[...].astype(F32) + dot(pick[...], flat(ret[...]), 0, 0)).astype(BF16)

    def cols(quarter):
        return pl.ds(pl.multiple_of(quarter * q, 128), q)

    mine = resid.at[:, cols(c)]
    to_far = push(resq, mine, gs.at[0], gr.at[0], (me, far))
    to_near = push(resq, mine, gs.at[1], gr.at[1], (me, near))
    to_far.start()
    to_near.start()
    resid[:, cols(c)] = resq[...]
    spot = resid.at[:, cols(far)]
    push(resq, spot, gs.at[0], gr.at[0], (me, far)).wait_recv()
    onward = push(spot, spot, gs.at[2], gr.at[2], (me, near))
    onward.start()
    push(resq, resid.at[:, cols(near)], gs.at[1], gr.at[1], (me, near)).wait_recv()
    push(resq, resid.at[:, cols(near_far)], gs.at[2], gr.at[2], (me, near)).wait_recv()

    for cp in (to_far, to_near, onward):
        cp.wait_send()

    def drain(k, carry):
        far_copy(k, c).wait_send()
        near_copy(k, c).wait_send()
        relay_copy(k, far).wait_send()
        part_copy(k, 0).wait_send()
        part_copy(k, 1).wait_send()
        x_copy(k).wait_send()

        @pl.when(k > 0)
        def _():
            out_copy(k).wait_send()
            home_copy(k).wait_send()
            tot_copy(k).wait_send()
            peer = source(k)
            push(tot, tot_out.at[peer], tssem.at[k], trsem.at[k], (peer, c)).wait_recv()

        return carry

    lax.fori_loop(0, n_sp, drain, 0)
    own_tot.wait()
    chain.finish()
    for cp in stores:
        cp.wait()


def experts(pack, pick, og_q, gate_weight, up_weight, down_weight, tot, state, n_tp):
    n_sp, _, cap, q = pack.shape
    tokens = og_q.shape[0]
    width = q * n_tp
    hid = gate_weight.shape[2]
    dma = pltpu.SemaphoreType.DMA
    block = pltpu.VMEM((n_sp, cap, q), BF16)
    vmem = pltpu.VMEM
    return pl.pallas_call(
        functools.partial(experts_kernel, n_sp, n_tp),
        out_shape=(
            jax.ShapeDtypeStruct(gate_weight.shape, BF16),
            jax.ShapeDtypeStruct(up_weight.shape, BF16),
            jax.ShapeDtypeStruct(down_weight.shape, BF16),
            jax.ShapeDtypeStruct((tokens, width), BF16),
            jax.ShapeDtypeStruct((n_sp,) + tot.shape, tot.dtype),
            jax.ShapeDtypeStruct((n_sp,) + state.shape, state.dtype),
        ),
        in_specs=vmem_specs(3) + any_specs(5),
        out_specs=tuple(any_specs(3) + vmem_specs(1) + any_specs(2)),
        scratch_shapes=[
            vmem((n_sp, n_tp, 2, cap, q), BF16),
            vmem((width, 2 * hid), BF16),
            vmem((hid, width), BF16),
            vmem((n_sp, cap, hid), BF16),
            vmem((n_sp, cap, 2 * hid), BF16),
            vmem((n_sp, n_tp, cap, q), BF16),
            vmem((2, n_sp, cap, q), BF16),
            block, block, block, block,
            vmem((tokens, q), BF16),
            vmem((width, hid), BF16),
            vmem((width, hid), BF16),
            vmem((hid, width), BF16),
            dma((3,)), dma((3,)), dma((1,)),
        ]
        + [dma((n_sp,))] * 8
        + [dma((2, n_sp))] * 2
        + [dma((n_sp,))] * 4
        + [dma((3,))] * 2
        + [dma((n_sp,))] * 2
        + chain_sems(n_sp),
        compiler_params=pltpu.CompilerParams(
            collective_id=0, has_side_effects=True, vmem_limit_bytes=56 * 2**20
        ),
        name="experts",
    )(pack, pick, og_q, gate_weight, up_weight, down_weight, tot, state)


def swap_kernel(
    n_sp, w, resid, state, normed, cols_out, states, normed_all, own_sem, ssem, rsem, *chain_sem
):
    me = lax.axis_index("sp")
    c = lax.axis_index("tp")
    greet(n_sp, me, c, True, ())

    def part(index):
        if len(resid.shape) == 3:
            return resid.at[index]
        return resid.at[:, pl.ds(pl.multiple_of(index * w, 128), w)]

    chain = Chain(state, states, n_sp, me, c, chain_sem[:5], (1,))
    chain.start()
    spread = Chain(normed, normed_all, n_sp, me, c, chain_sem[5:], (0, 1))
    spread.start()
    waits = []

    def send(k):
        peer = lax.rem(me + k, n_sp)
        cp = push(part(peer), cols_out.at[me], ssem.at[k], rsem.at[k], (peer, c))
        cp.start()
        waits.append(cp)

    local = pltpu.make_async_copy(part(me), cols_out.at[me], own_sem.at[0])
    local.start()
    for d in range(1, n_sp // 2):
        send(2 * d)
        send(2 * d - 1)
        chain.step(d)
        spread.step(d)
    send(n_sp - 1)
    for k in range(1, n_sp):
        source = lax.rem(me + n_sp - k, n_sp)
        spot = cols_out.at[source]
        push(spot, spot, ssem.at[k], rsem.at[k], (source, c)).wait_recv()
    for cp in waits:
        cp.wait_send()
    local.wait()
    chain.finish()
    spread.finish()


def swap(resid, state, normed, n_sp):
    tokens, width = resid.shape
    w = width // n_sp
    if w % 128:
        resid = resid.reshape(tokens, n_sp, w).transpose(1, 0, 2)
    dma = pltpu.SemaphoreType.DMA
    return pl.pallas_call(
        functools.partial(swap_kernel, n_sp, w),
        out_shape=(
            jax.ShapeDtypeStruct((n_sp, tokens, w), BF16),
            jax.ShapeDtypeStruct((n_sp,) + state.shape, BF16),
            jax.ShapeDtypeStruct((n_sp,) + normed.shape, BF16),
        ),
        in_specs=any_specs(3),
        out_specs=tuple(any_specs(3)),
        scratch_shapes=[dma((1,)), dma((n_sp,)), dma((n_sp,))] + chain_sems(n_sp) * 2,
        compiler_params=pltpu.CompilerParams(collective_id=2, has_side_effects=True),
        name="swap",
    )(resid, state, normed)


def rotation_tables(start, count, key_width):
    frequency = 1.0 / 10000.0 ** jnp.linspace(0.0, 1.0, key_width // 2, dtype=F32)
    frequency = jnp.repeat(frequency, 2)
    token_position = (start + jnp.arange(count, dtype=jnp.int32)).astype(F32)
    angles = token_position[:, None] * frequency[None, :]
    return (jnp.cos(angles)[None], jnp.sin(angles)[None])


def swap_matrix(key_width):
    row = jnp.arange(key_width)[:, None]
    col = jnp.arange(key_width)[None, :]
    up = (col == row + 1) & (row % 2 == 0)
    down = (col == row - 1) & (row % 2 == 1)
    return (up.astype(F32) - down.astype(F32)).astype(BF16)


def turn(field, cosines, sines, matrix):
    turned = jnp.einsum("htk,kl->htl", field.astype(BF16), matrix, preferred_element_type=F32)
    return field.astype(F32) * cosines + turned * sines


def ein(spec, a, b):
    return jnp.einsum(spec, a.astype(BF16), b.astype(BF16), preferred_element_type=F32)


def fine(spec, a, b):
    return jnp.einsum(spec, a.astype(F32), b.astype(F32), precision=lax.Precision.HIGHEST)


def weighted(states, factors, present):
    kept = jnp.where(present[:, None, None, None], states.astype(F32), 0.0)
    return jnp.sum(kept * factors[:, :, None, None], axis=0)


def mm(a, b, da, db):
    return lax.dot_general(a, b, (((da,), (db,)), ((), ())), preferred_element_type=F32)


def per_device(
    stream, out_grad, routes, route_weight, queries, key_vectors, value_vectors, log_decay,
    out_proj, gate_weight, up_weight, down_weight,
):
    n_sp = lax.axis_size("sp")
    n_tp = lax.axis_size("tp")
    me = lax.axis_index("sp")
    tokens, width = stream.shape
    capacity = 4 * tokens // n_sp
    slots = n_sp * capacity
    quarter = width // n_tp
    heads = queries.shape[1]
    key_width = queries.shape[2]
    value_width = value_vectors.shape[2]

    ids = jnp.arange(n_sp, dtype=jnp.int32)
    chosen = routes[:, :, None] == ids[None, None, :]
    counts = jnp.sum(chosen.astype(F32), axis=1).astype(BF16)
    place = jnp.arange(tokens)
    lower = (place[:, None] > place[None, :]).astype(BF16)
    before = jnp.dot(lower, counts, preferred_element_type=F32)
    slot = jnp.sum(jnp.where(chosen, before[:, None, :], 0.0), axis=2).astype(jnp.int32)
    target = routes * capacity + slot
    spots = jnp.arange(slots, dtype=jnp.int32)
    hit = target.T[:, None, :] == spots[None, :, None]
    pick = (hit[0] | hit[1]).astype(BF16)
    weight = jnp.sum(
        jnp.where(hit[0], route_weight[None, :, 0], 0.0)
        + jnp.where(hit[1], route_weight[None, :, 1], 0.0),
        axis=1,
    )
    col_start = lax.axis_index("tp") * quarter
    stream_q = lax.dynamic_slice_in_dim(stream, col_start, quarter, 1)
    og_q = lax.dynamic_slice_in_dim(out_grad, col_start, quarter, 1)
    send_rows = jnp.dot(pick, stream_q, preferred_element_type=F32).astype(BF16)
    send_grads = (
        weight[:, None] * jnp.dot(pick, og_q, preferred_element_type=F32)
    ).astype(BF16)

    running = jnp.cumsum(log_decay, axis=0).T
    block_total = running[:, -1]
    tot = jnp.broadcast_to(jnp.pad(block_total, (0, 128 - heads))[None, :], (8, 128))
    matrix = swap_matrix(key_width)
    cosines, sines = rotation_tables(me * tokens, tokens, key_width)
    scale = key_width ** (-0.5)
    query_rot = turn(queries.transpose(1, 0, 2), cosines, sines, matrix)
    key_rot = turn(key_vectors.transpose(1, 0, 2), cosines, sines, matrix) * scale
    values = value_vectors.transpose(1, 0, 2)
    causal = (place[:, None] >= place[None, :])[None]
    difference = running[:, :, None] - running[:, None, :]
    mask = jnp.where(causal, jnp.exp(jnp.where(causal, difference, 0.0)), 0.0)
    decay = jnp.exp(running)[..., None]
    remaining = jnp.exp(block_total[:, None] - running)[..., None]
    inner = ein("wfs,wfi->wsi", key_rot * remaining, values).astype(BF16)
    pack = jnp.stack(
        [send_rows.reshape(n_sp, capacity, quarter), send_grads.reshape(n_sp, capacity, quarter)],
        axis=1,
    )
    gate_part, up_part, down_part, resid, tots, inner_all = experts(
        pack, pick, og_q, gate_weight, up_weight, down_weight, tot, inner, n_tp
    )
    key_bf = key_rot.astype(BF16)
    query_bf = query_rot.astype(BF16)
    weights = fine("hik,hjk->hij", query_rot, key_rot) * mask
    retained_local = fine("hij,hjv->hiv", weights, values)

    totals = tots[:, 0, :heads]
    sums = jnp.cumsum(totals, axis=0)
    sum_before = jnp.sum(jnp.where((ids < me)[:, None], totals, 0.0), axis=0)
    sum_through = sum_before + block_total
    past = jnp.where((ids < me)[:, None], sum_before[None] - sums, 0.0)
    past = jnp.where((ids < me)[:, None], jnp.exp(past), 0.0)
    coming = jnp.where((ids > me)[:, None], sums - totals - sum_through[None], 0.0)
    coming = jnp.where((ids > me)[:, None], jnp.exp(coming), 0.0)
    incoming = weighted(inner_all, past, ids < me)
    retained = retained_local + decay * fine("dzr,drs->dzs", query_rot, incoming)
    inverse_rms = lax.rsqrt(jnp.mean(retained * retained, axis=-1, keepdims=True) + EPSILON)
    normed = retained * inverse_rms
    normed_bf = normed.transpose(1, 0, 2).reshape(tokens, heads * value_width).astype(BF16)

    normed_grad = jnp.dot(resid, out_proj, preferred_element_type=F32)
    normed_grad = normed_grad.reshape(tokens, heads, value_width).transpose(1, 0, 2)
    grad = inverse_rms * (
        normed_grad - normed * jnp.mean(normed_grad * normed, axis=-1, keepdims=True)
    )
    grad_bf = grad.astype(BF16)
    inner_grad = ein("gwn,gwj->gnj", query_rot * decay, grad_bf).astype(BF16)
    resid_cols, grads_all, normed_all = swap(resid, inner_grad, normed_bf, n_sp)
    future = weighted(grads_all, coming, ids > me).astype(BF16)
    score = fine("hiv,hjv->hij", grad, values) * mask
    query_portion = ein("hij,hjk->hik", score, key_bf) + decay * fine(
        "bpl,btl->bpt", grad, incoming
    )
    key_portion = ein("hij,hik->hjk", score, query_bf) + remaining * ein(
        "uxn,ubn->uxb", values, future
    )
    value_portion = ein("hij,hiv->hjv", weights, grad_bf) + remaining * ein(
        "bui,bim->bum", key_bf, future
    )
    query_grad = turn(query_portion, cosines, -sines, matrix).astype(BF16).transpose(1, 0, 2)
    key_grad = (
        (turn(key_portion, cosines, -sines, matrix) * scale).astype(BF16).transpose(1, 0, 2)
    )
    value_grad = value_portion.astype(BF16).transpose(1, 0, 2)
    proj_grad = mm(
        resid_cols.reshape(n_sp * tokens, -1), normed_all.reshape(n_sp * tokens, -1), 0, 0
    )
    return (
        gate_part,
        up_part,
        down_part,
        proj_grad,
        query_grad,
        key_grad,
        value_grad,
    )


def solution(mesh):
    in_specs = (
        P("sp", None),
        P("sp", None),
        P("sp", None),
        P("sp", None),
        P("sp", "tp", None),
        P("sp", "tp", None),
        P("sp", "tp", None),
        P("sp", "tp"),
        P(None, "tp"),
        P("sp", None, "tp"),
        P("sp", None, "tp"),
        P("sp", "tp", None),
    )
    out_specs = (
        P("sp", None, "tp"),
        P("sp", None, "tp"),
        P("sp", "tp", None),
        P("sp", "tp"),
        P("sp", "tp", None),
        P("sp", "tp", None),
        P("sp", "tp", None),
    )
    return jax.shard_map(
        per_device, mesh=mesh, in_specs=in_specs, out_specs=out_specs, check_vma=False
    )
```

time: 167 us -> 155 us (0.928)
  matrix products: 28.6 us -> 12.5 us
  Pallas kernels: 113 us -> 116 us
  local copies, waits for them, and re-layouts: 13.9 us -> 15.8 us
    dot_general x9 -> x1, matrix products: 15.3 us -> 2.78 us  [mm(): lax.dot_general(a, b, (((da,), (db,)), ((), ())), preferred_element_type=...]
    pallas_call x1, Pallas kernels: 31.3 us -> 38.9 us  [swap(): pl.pallas_call(functools.partial(swap_kernel, n_sp, w), out_shape=(jax.Sh...]
    pallas_call x2 -> x1, Pallas kernels: 81.9 us -> 77.4 us  [experts(): pl.pallas_call(functools.partial(experts_kernel, n_sp, n_tp), out_shape=(...]
    unnamed x58 -> x61, local copies, waits for them, and re-layouts: 6.61 us -> 7.93 us
where the time goes in v1:
time: 155 us
  Pallas kernels  116 us (75%)
  local copies, waits for them, and re-layouts  15.8 us (10%)
  matrix products  12.5 us (8%)
  other arithmetic  8.88 us (6%)
    pallas_call x1, Pallas kernels, experts(): pl.pallas_call(functools.partial(experts_kernel, n_sp, n_tp), out_shape=(...  77.4 us
    pallas_call x1, Pallas kernels, swap(): pl.pallas_call(functools.partial(swap_kernel, n_sp, w), out_shape=(jax.Sh...  38.9 us
    unnamed x61, local copies, waits for them, and re-layouts  7.93 us

profile of v1, /device:TPU:0, one launch (start us, length us, event | category | flops | bytes accessed | tf_op | source)
XLA Modules:
  0.0 154.6 jit_solution(17786750961061277196)
XLA Ops:
  0.8 0.8 slice_bitcast_fusion.3
  1.7 0.7 convert_reduce_fusion
  2.5 0.7 select_reduce_fusion
  3.2 0.7 add_bitcast_fusion
  4.1 1.0 copy.206
  5.1 1.0 copy.202
  6.1 0.8 copy.200
  8.6 0.6 copy.230
  9.2 0.7 copy.217
  10.1 0.9 constant_dynamic-slice_fusion.og
  11.0 0.7 fusion.68.pick
  12.9 0.8 convolution_convert_fusion.2.state
  14.5 1.2 convolution_convert_fusion
  15.7 1.1 pad_maximum_fusion.pack
  16.8 77.4 %experts.1 = (bf16[1,2048,256]{2,1,0:T(8,128)(2,1)}, bf16[1,2048,256]{2,1,0:T(8,128)(2,1)}, bf16[1,256,2048]{2,1,0:T(8,128)(2,1)}, bf16[128,2048]{1,0:T(8,128)(2...) custom-call(bf16[8,2,64,512]{3,2,1,0:T(8,128)(2,1)} %pad_maximum_fusion.pack, bf16[512,128]{1,0:T(8,128)(2,1)} %fusion.68.pick, ...), custom_call_target="tpu_custom_call" | custom-call | tf_op jit(solution)/shard_map/experts/pallas_call | solution.py:392
  94.2 0.8 slice.25
  95.4 0.7 copy.231
  96.2 1.6 %multiply_reduce_fusion.1 = f32[2,128,256]{2,1,0:T(8,128)S(1)} fusion(bf16[8,2,128,256]{3,2,1,0:T(8,128)(2,1)} %get-tuple-element.20, f32[8,2]{1,0:T(8,128)S(1)} %copy.213, pred[8]{0:T(512)(128)(4,1)S(1)} %get-tuple-element.80), kind=kLoop, calls=%fused_computation.1 | loop fusion | flops 2031616 | bytes 1310792 | tf_op jit(solution)/shard_map/reduce_sum | solution.py:527
  98.3 1.7 %fusion.72 = f32[128,512]{0,1:T(8,128)} fusion(bf16[128,2048]{1,0:T(8,128)(2,1)S(1)} %copy-done.1, bf16[2048,512]{1,0:T(8,128)(2,1)S(1)} %copy-done), kind=kOutput, calls=%fused_computation.132 | convolution fusion | flops 268435456 | bytes 2883584 | tf_op jit(solution)/shard_map/dot_general | solution.py:614
  99.9 1.1 copy.216
  101.0 1.0 multiply_reduce_fusion.2
  102.1 0.8 fusion.22
  102.9 0.7 copy.263
  105.1 0.8 convolution_convert_fusion.1.state
  106.7 0.7 copy.238
  107.4 38.9 %swap.1 = (bf16[8,128,256]{2,1,0:T(8,128)(2,1)}, bf16[8,2,128,256]{3,2,1,0:T(8,128)(2,1)}, bf16[8,128,512]{2,1,0:T(8,128)(2,1)}) custom-call(bf16[128,2048]{1,0:T(8,128)(2,1)} %get-tuple-element.19.resid, bf16[2,128,256]{2,1,0:T(8,128)(2,1)} %convolution_convert_fusion.1.state, bf16[128,512]{1,0:T(8,128)(2,1)} %bitcast.167), custom_call_target="tpu_custom_call" | custom-call | tf_op jit(solution)/shard_map/swap/pallas_call | solution.py:481
  146.3 2.8 %convolution_bitcast_fusion = f32[256,512]{1,0:T(8,128)} fusion(bf16[8,128,256]{2,1,0:T(8,128)(2,1)} %get-tuple-element.22, bf16[8,128,512]{2,1,0:T(8,128)(2,1)} %get-tuple-element.23), kind=kOutput, calls=%fused_computation.5 | convolution fusion | flops 268435456 | bytes 2097152 | tf_op jit(solution)/shard_map/dot_general | solution.py:531
  150.2 0.7 copy.239
  150.9 0.8 copy.240
  151.7 1.0 copy.278
  152.7 1.0 copy.279
  153.6 1.0 copy.280
  (101 shorter events, 8.5 us)
Async XLA Ops:
  0.6 97.6 %copy-start = (bf16[2048,512]{1,0:T(8,128)(2,1)S(1)}, bf16[2048,512]{1,0:T(8,128)(2,1)}, u32[]{:S(2)}) copy-start(bf16[2048,512]{1,0:T(8,128)(2,1)} %param.20) | copy-start | bytes 6291460
  0.6 12.3 %copy-start.2 = (bf16[128,2,256]{2,1,0:T(2,128)(2,1)S(1)}, bf16[128,2,256]{2,1,0:T(2,128)(2,1)}, u32[]{:S(2)}) copy-start(bf16[128,2,256]{2,1,0:T(2,128)(2,1)} %param.18) | copy-start | bytes 393220
  0.8 94.6 %copy-start.24 = (pred[8]{0:T(512)(128)(4,1)}, pred[8]{0:T(512)(128)(4,1)S(1)}, u32[]{:S(2)}) copy-start(pred[8]{0:T(512)(128)(4,1)S(1)} %get-tuple-element.79) | copy-start | bytes 28
  1.6 12.8 %copy-start.15 = (pred[128]{0:T(512)(128)(4,1)}, pred[128]{0:T(512)(128)(4,1)S(1)}, u32[]{:S(2)}) copy-start(pred[128]{0:T(512)(128)(4,1)S(1)} %get-tuple-element.77) | copy-start | bytes 388
  1.6 12.9 %copy-start.17 = (pred[128]{0:T(512)(128)(4,1)}, pred[128]{0:T(512)(128)(4,1)S(1)}, u32[]{:S(2)}) copy-start(pred[128]{0:T(512)(128)(4,1)S(1)} %get-tuple-element.78) | copy-start | bytes 388
  1.6 12.8 %copy-start.19 = (s32[128]{0:T(128)}, s32[128]{0:T(128)S(1)}, u32[]{:S(2)}) copy-start(s32[128]{0:T(128)S(1)} %get-tuple-element.81) | copy-start | bytes 1540
  1.7 12.8 %copy-start.21 = (s32[128]{0:T(128)}, s32[128]{0:T(128)S(1)}, u32[]{:S(2)}) copy-start(s32[128]{0:T(128)S(1)} %get-tuple-element.82) | copy-start | bytes 1540
  7.1 8.6 %copy-start.8 = (f32[128,2]{0,1:T(2,128)}, f32[128,2]{0,1:T(2,128)S(1)}, u32[]{:S(2)}) copy-start(f32[128,2]{0,1:T(2,128)S(1)} %copy.201) | copy-start | bytes 3076
  11.0 5.8 %copy-start.7 = (bf16[128,512]{1,0:T(8,128)(2,1)}, bf16[128,512]{1,0:T(8,128)(2,1)S(1)}, u32[]{:S(2)}) copy-start(bf16[128,512]{1,0:T(8,128)(2,1)S(1)} %constant_dynamic-slice_fusion.og) | copy-start | bytes 393220
  96.2 2.1 %copy-start.1 = (bf16[128,2048]{1,0:T(8,128)(2,1)S(1)}, bf16[128,2048]{1,0:T(8,128)(2,1)}, u32[]{:S(2)}) copy-start(bf16[128,2048]{1,0:T(8,128)(2,1)} %get-tuple-element.19.resid) | copy-start | bytes 1572868
  101.0 3.3 %copy-start.9 = (f32[128,2]{0,1:T(2,128)S(1)}, f32[128,2]{0,1:T(2,128)}, u32[]{:S(2)}) copy-start(f32[128,2]{0,1:T(2,128)} %copy-done.8) | copy-start | bytes 3076
  102.1 3.0 %copy-start.11 = (f32[2,128]{1,0:T(2,128)S(1)}, f32[2,128]{1,0:T(2,128)}, u32[]{:S(2)}) copy-start(f32[2,128]{1,0:T(2,128)} %get-tuple-element.73) | copy-start | bytes 3076
  103.8 2.6 %copy-start.12 = (f32[2,128]{1,0:T(2,128)S(1)}, f32[2,128]{1,0:T(2,128)}, u32[]{:S(2)}) copy-start(f32[2,128]{1,0:T(2,128)} %get-tuple-element.73) | copy-start | bytes 3076
  103.8 2.6 %copy-start.14 = (f32[128,2]{0,1:T(2,128)S(1)}, f32[128,2]{0,1:T(2,128)}, u32[]{:S(2)}) copy-start(f32[128,2]{0,1:T(2,128)} %copy.217) | copy-start | bytes 3076
  103.8 2.6 %copy-start.16 = (pred[128]{0:T(512)(128)(4,1)S(1)}, pred[128]{0:T(512)(128)(4,1)}, u32[]{:S(2)}) copy-start(pred[128]{0:T(512)(128)(4,1)} %copy-done.15) | copy-start | bytes 388
  103.8 2.6 %copy-start.18 = (pred[128]{0:T(512)(128)(4,1)S(1)}, pred[128]{0:T(512)(128)(4,1)}, u32[]{:S(2)}) copy-start(pred[128]{0:T(512)(128)(4,1)} %copy-done.17) | copy-start | bytes 388
  103.8 2.6 %copy-start.20 = (s32[128]{0:T(128)S(1)}, s32[128]{0:T(128)}, u32[]{:S(2)}) copy-start(s32[128]{0:T(128)} %copy-done.19) | copy-start | bytes 1540
  103.8 2.6 %copy-start.22 = (s32[128]{0:T(128)S(1)}, s32[128]{0:T(128)}, u32[]{:S(2)}) copy-start(s32[128]{0:T(128)} %copy-done.21) | copy-start | bytes 1540
  106.1 43.0 %copy-start.10 = (f32[8,2]{1,0:T(8,128)S(1)}, f32[8,2]{1,0:T(8,128)}, u32[]{:S(2)}) copy-start(f32[8,2]{1,0:T(8,128)} %copy.231) | copy-start | bytes 196
  106.1 43.0 %copy-start.25 = (pred[8]{0:T(512)(128)(4,1)S(1)}, pred[8]{0:T(512)(128)(4,1)}, u32[]{:S(2)}) copy-start(pred[8]{0:T(512)(128)(4,1)} %copy-done.24) | copy-start | bytes 28
  106.7 42.7 %copy-start.13 = (f32[128,2]{0,1:T(2,128)S(1)}, f32[128,2]{0,1:T(2,128)}, u32[]{:S(2)}) copy-start(f32[128,2]{0,1:T(2,128)} %copy.230) | copy-start | bytes 3076
  146.3 2.8 %copy-start.6 = (bf16[8,2,128,256]{3,2,1,0:T(8,128)(2,1)S(1)}, bf16[8,2,128,256]{3,2,1,0:T(8,128)(2,1)}, u32[]{:S(2)}) copy-start(bf16[8,2,128,256]{3,2,1,0:T(8,128)(2,1)} %get-tuple-element.24) | copy-start | bytes 3145732
  146.3 3.6 %copy-start.23 = (f32[2,128]{1,0:T(2,128)S(1)}, f32[2,128]{1,0:T(2,128)}, u32[]{:S(2)}) copy-start(f32[2,128]{1,0:T(2,128)} %get-tuple-element.63) | copy-start | bytes 3076
  146.3 5.4 %copy-start.5 = (bf16[1,2048,256]{2,1,0:T(8,128)(2,1)S(1)}, bf16[1,2048,256]{2,1,0:T(8,128)(2,1)}, u32[]{:S(2)}) copy-start(bf16[1,2048,256]{2,1,0:T(8,128)(2,1)} %get-tuple-element.90) | copy-start | bytes 3145732
  149.5 3.2 %copy-start.4 = (bf16[1,2048,256]{2,1,0:T(8,128)(2,1)S(1)}, bf16[1,2048,256]{2,1,0:T(8,128)(2,1)}, u32[]{:S(2)}) copy-start(bf16[1,2048,256]{2,1,0:T(8,128)(2,1)} %get-tuple-element.91) | copy-start | bytes 3145732
  151.7 1.9 %copy-start.3 = (bf16[1,256,2048]{2,1,0:T(8,128)(2,1)S(1)}, bf16[1,256,2048]{2,1,0:T(8,128)(2,1)}, u32[]{:S(2)}) copy-start(bf16[1,256,2048]{2,1,0:T(8,128)(2,1)} %get-tuple-element.92) | copy-start | bytes 3145732

commit v2 on v1

v2 whole, which is shorter than its diff:
```python
import functools

import jax
import jax.numpy as jnp
import numpy as np
from jax import lax
from jax.experimental import pallas as pl
from jax.experimental.pallas import tpu as pltpu
from jax.sharding import PartitionSpec as P

CLAMP_LIMIT = 7.0
GATE_SLOPE = 1.702
EPSILON = 1e-06
F32 = jnp.float32
BF16 = jnp.bfloat16
MESH = pl.DeviceIdType.MESH
SPLIT = 2


def any_specs(count):
    return [pl.BlockSpec(memory_space=pl.ANY)] * count


def vmem_specs(count):
    return [pl.BlockSpec(memory_space=pltpu.VMEM)] * count


def push(src, dst, send_sem, recv_sem, device):
    return pltpu.make_async_remote_copy(
        src_ref=src,
        dst_ref=dst,
        send_sem=send_sem,
        recv_sem=recv_sem,
        device_id=device,
        device_id_type=MESH,
    )


class Chain:
    def __init__(self, src, out, n_sp, me, c, sems, ways):
        self.src, self.out, self.me, self.c = src, out, me, c
        self.pairs, self.ways = n_sp // 2, ways
        self.pair = me // 2
        self.other = me + 1 - 2 * lax.rem(me, 2)
        self.zs, self.zr, self.ys, self.yr = sems

    def has(self, d, way):
        return self.pair >= d if way == 0 else self.pair + d < self.pairs

    def room(self, way):
        return self.pair + 1 < self.pairs if way == 0 else self.pair >= 1

    def spot(self, base, d, way):
        return self.out.at[base - 2 * d if way == 0 else base + 2 * d]

    def along(self, d, way):
        spot = self.spot(self.me, d, way)
        return push(
            self.src if d == 0 else spot, spot, self.zs.at[way, d], self.zr.at[way, d + 1],
            (self.me + 2 if way == 0 else self.me - 2, self.c),
        )

    def across(self, d, way):
        spot = self.spot(self.me, d, way)
        return push(
            self.src if d == 0 else spot, spot, self.ys.at[way, d], self.yr.at[way, d],
            (self.other, self.c),
        )

    def each(self, d, act):
        for way in self.ways:

            @pl.when(self.has(d, way))
            def _():
                if d < self.pairs - 1:

                    @pl.when(self.room(way))
                    def _():
                        act(self.along(d, way))

                if d > 0 or way == self.ways[0]:
                    act(self.across(d, way))

    def start(self):
        self.each(0, lambda cp: cp.start())

    def step(self, d):
        for way in self.ways:

            @pl.when(self.has(d, way))
            def _():
                spot = self.spot(self.me, d, way)
                push(
                    spot, spot, self.zs.at[way, d], self.zr.at[way, d], (self.other, self.c)
                ).wait_recv()

        self.each(d, lambda cp: cp.start())

    def finish(self):
        for d in range(self.pairs):
            for way in self.ways:
                if d == 0 and way != self.ways[0]:
                    continue

                @pl.when(self.has(d, way))
                def _():
                    spot = self.spot(self.other, d, way)
                    push(
                        spot, spot, self.ys.at[way, d], self.yr.at[way, d], (self.other, self.c)
                    ).wait_recv()

            self.each(d, lambda cp: cp.wait_send())


class Scan:
    def __init__(self, forward, n_sp, me, c, bufs, sems, totals, heads):
        self.forward, self.me, self.c = forward, me, c
        self.zin, self.zout, self.min, self.mout = bufs
        self.zs, self.zr, self.ms, self.mr = sems
        self.own_tot, self.other_tot = totals
        pairs = n_sp // 2
        pair = me // 2
        parity = lax.rem(me, 2)
        self.other = me + 1 - 2 * parity
        self.prev = pair > 0 if forward else pair + 1 < pairs
        self.next = pair + 1 < pairs if forward else pair > 0
        self.ahead = me + 2 if forward else me - 2
        self.slot = pair if forward else pairs - 1 - pair
        self.inside = jnp.where(parity == (0 if forward else 1), 1.0, 0.0)
        self.count = heads * SPLIT

    def z_copy(self, j):
        return push(
            self.zout.at[j], self.zin.at[j], self.zs.at[j], self.zr.at[j], (self.ahead, self.c)
        )

    def m_copy(self, j):
        return push(
            self.mout.at[j], self.min.at[j], self.ms.at[j], self.mr.at[j], (self.other, self.c)
        )

    def clear(self):
        @pl.when(jnp.logical_not(self.prev))
        def _():
            self.zin[...] = jnp.zeros_like(self.zin)

    def decays(self, j):
        h = j // SPLIT
        return jnp.exp(self.own_tot[h, 0:1, 0:1]), jnp.exp(self.other_tot[h, 0:1, 0:1])

    def step(self, own):
        s = self.inside
        for j in range(self.count):
            mine, others = self.decays(j)

            @pl.when(self.prev)
            def _():
                self.z_copy(j).wait_recv()

            z = self.zin[j].astype(F32)
            i = own[j]
            self.zout[j] = (mine * others * z + (s * others + (1.0 - s)) * i).astype(BF16)

            @pl.when(self.next)
            def _():
                self.z_copy(j).start()

            self.mout[j] = ((s * mine + (1.0 - s)) * z + s * i).astype(BF16)
            self.m_copy(j).start()

    def result(self, j):
        s = self.inside
        others = self.decays(j)[1]
        self.m_copy(j).wait_recv()
        z = self.zin[j].astype(F32)
        return (self.min[j].astype(F32) + (s + (1.0 - s) * others) * z).astype(BF16)

    def finish(self):
        for j in range(self.count):

            @pl.when(self.next)
            def _():
                self.z_copy(j).wait_send()

            self.m_copy(j).wait_send()


def dot(a, b, da, db):
    return lax.dot_general(a, b, (((da,), (db,)), ((), ())), preferred_element_type=F32)


def flat(block):
    n, cap, q = block.shape
    if cap % 16 == 0:
        return block.reshape(n * cap, q)
    return block.astype(F32).reshape(n * cap, q).astype(BF16)


def swapped(x):
    width = x.shape[1]
    even = lax.rem(lax.broadcasted_iota(jnp.int32, x.shape, 1), 2) == 0
    return jnp.where(even, -pltpu.roll(x, width - 1, 1), pltpu.roll(x, 1, 1))


def whole_kernel(
    n_sp, n_tp, heads,
    stream, og, routes, route_w, queries, keys, values, log_decay, cos_t, sin_t, cos_s, sin_s,
    gate_w, up_w, down_w, proj_w,
    gate_o, up_o, down_o, proj_o, query_o, key_o, value_o,
    full, pack, gu, dw, pw, act, gug, back, part, xbuf, xrecv, sendbuf, ret, gout, uout, dout,
    pick, wcol, slotmap, weight_map, resid, rcols, normed_own, normed_all, normed_f, inv, dec, rem_,
    mask, wts, qr, kr, cosb, sinb, totb, toto, inner, inner_g, incoming, proj,
    fzin, fzout, fmin, fmout, bzin, bzout, bmin, bmout,
    wsem, osem, tsem, ssem, rsem, fs, fr, ns, nr, es, er, ps, pr, xs, xr, hs, hr, gs, gr,
    cs, cr, ds, dr, *more,
):
    fsem, bsem, chain_sem = more[0:4], more[4:8], more[8:12]
    me = lax.axis_index("sp")
    c = lax.axis_index("tp")
    core, plane = lax.rem(c, 2), c // 2
    ocore, oplane = 1 - core, 1 - plane
    far = lax.rem(c + n_tp // 2, n_tp)
    near = c + 1 - 2 * core
    other = me + 1 - 2 * lax.rem(me, 2)
    cap, q = full.shape[4:]
    hid = dw.shape[0]
    tokens = stream.shape[0]
    kd = cos_t.shape[1]
    vd = values.shape[1] // heads
    scale = kd ** (-0.5)
    bits = [1 << b for b in range((n_sp - 1).bit_length())]

    def peer(k):
        out = 0
        for b in bits:
            out = out + b * lax.rem(me // b + k // b, 2)
        return out

    loads = [
        pltpu.make_async_copy(gate_w.at[0], gu.at[:, pl.ds(0, hid)], wsem.at[0]),
        pltpu.make_async_copy(up_w.at[0], gu.at[:, pl.ds(hid, hid)], wsem.at[1]),
        pltpu.make_async_copy(down_w.at[0], dw, wsem.at[2]),
        pltpu.make_async_copy(proj_w, pw, wsem.at[3]),
    ]
    for cp in loads:
        cp.start()
    barrier = pltpu.get_barrier_semaphore()

    def hello(k, carry):
        pl.semaphore_signal(barrier, inc=1, device_id=(peer(k), c), device_id_type=MESH)
        return carry

    lax.fori_loop(1, n_sp, hello, 0)
    for t in (far, near):
        pl.semaphore_signal(barrier, inc=1, device_id=(me, t), device_id_type=MESH)

    def cols(index):
        return pl.ds(pl.multiple_of(index * q, 128), q)

    expert = lax.broadcasted_iota(jnp.int32, (n_sp, tokens), 0)
    first_of = expert == routes[0:1, :]
    second_of = expert == routes[1:2, :]
    chosen = first_of | second_of
    weight_map[...] = jnp.where(first_of, route_w[0:1, :], 0.0) + jnp.where(
        second_of, route_w[1:2, :], 0.0
    )
    row = lax.broadcasted_iota(jnp.int32, (tokens, tokens), 0)
    col = lax.broadcasted_iota(jnp.int32, (tokens, tokens), 1)
    earlier = jnp.where(row < col, 1.0, 0.0).astype(BF16)
    before = dot(jnp.where(chosen, 1.0, 0.0).astype(BF16), earlier, 1, 0)
    slotmap[...] = jnp.where(chosen, before, -1.0)
    place = lax.broadcasted_iota(jnp.int32, (cap, tokens), 0).astype(F32)
    for e in range(n_sp):
        hit = jnp.where(slotmap[e : e + 1, :] == place, 1.0, 0.0)
        pick[e] = hit.astype(BF16)
        wcol[e] = jnp.sum(hit * weight_map[e : e + 1, :], axis=1, keepdims=True)

    def fill(spot, e, index):
        rows = dot(pick[e], stream[:, cols(index)], 1, 0)
        grads = wcol[e] * dot(pick[e], og[:, cols(index)], 1, 0)
        spot[0] = rows.astype(BF16)
        spot[1] = grads.astype(BF16)

    def out_copy(k):
        return push(
            pack.at[k, plane], full.at[me, core, plane], ssem.at[k], rsem.at[k], (peer(k), c)
        )

    def out_pair():
        return push(pack.at[1], full.at[me, core], ssem.at[1], rsem.at[1], (peer(1), c))

    def far_copy(k, p):
        spot = full.at[peer(k), core, p]
        return push(spot, spot, fs.at[k], fr.at[k], (me, far))

    def near_copy(k, side):
        spot = full.at[peer(k), side, plane]
        return push(spot, spot, ns.at[k], nr.at[k], (me, near))

    def near_pair(k, side):
        spot = full.at[peer(k), side]
        return push(spot, spot, ns.at[k], nr.at[k], (me, near))

    def relay_copy(k, side):
        spot = full.at[peer(k), side, oplane]
        return push(spot, spot, es.at[k], er.at[k], (me, near))

    def part_copy(k):
        return push(back.at[k, ocore], part.at[k], ps.at[k], pr.at[k], (me, near))

    def x_copy(k):
        return push(xbuf.at[k], xrecv.at[k], xs.at[k], xr.at[k], (me, far))

    def home_copy(k):
        return push(sendbuf.at[k], ret.at[k], hs.at[k], hr.at[k], (peer(k), c))

    fill(pack.at[1, plane], peer(1), c)
    fill(pack.at[1, oplane], peer(1), far)
    fill(pack.at[2, plane], peer(2), c)
    pl.semaphore_wait(barrier, n_sp - 1 + 2)
    out_pair().start()

    def send_out(k, carry):
        @pl.when(k < n_sp)
        def _():
            fill(pack.at[k, plane], peer(k), c)

        out_copy(k - 1).start()
        return carry

    lax.fori_loop(3, n_sp + 1, send_out, 0)
    fill(full.at[me, core, plane], me, c)
    fill(full.at[me, core, oplane], me, far)

    lower = jnp.where(row >= col, 1.0, 0.0)
    running = lax.dot_general(
        lower, log_decay[...], (((1,), (0,)), ((), ())), preferred_element_type=F32,
        precision=lax.Precision.HIGHEST,
    )
    for h in range(heads):
        totb[h] = jnp.broadcast_to(running[tokens - 1 : tokens, h : h + 1], totb.shape[1:])
    near_pair(0, core).start()
    start_cos, start_sin = cos_s[pl.ds(me, 1), :], sin_s[pl.ds(me, 1), :]
    cosines = start_cos * cos_t[...] - start_sin * sin_t[...]
    sines = start_sin * cos_t[...] + start_cos * sin_t[...]
    cosb[...] = cosines
    sinb[...] = sines
    swap_tot = push(totb, toto, tsem.at[0], tsem.at[1], (other, c))
    swap_tot.start()
    rows_of = kd // SPLIT
    for h in range(heads):
        x = queries[:, h * kd : (h + 1) * kd].astype(F32)
        qr[h] = (x * cosines + swapped(x) * sines).astype(BF16)
        x = keys[:, h * kd : (h + 1) * kd].astype(F32)
        key = (x * cosines + swapped(x) * sines) * scale
        kr[h] = key.astype(BF16)
        run = running[:, h : h + 1]
        left = jnp.exp(running[tokens - 1 : tokens, h : h + 1] - run)
        dec[h] = jnp.exp(run)
        rem_[h] = left
        state = dot((key * left).astype(BF16), values[:, h * vd : (h + 1) * vd], 0, 0)
        for s in range(SPLIT):
            inner[h * SPLIT + s] = state[s * rows_of : (s + 1) * rows_of]
        spread_run = jnp.broadcast_to(run, (tokens, tokens))
        difference = spread_run - spread_run.T
        causal = row >= col
        mask[h] = jnp.where(causal, jnp.exp(jnp.where(causal, difference, 0.0)), 0.0)
    totals = (totb, toto)
    past = Scan(True, n_sp, me, c, (fzin, fzout, fmin, fmout), fsem, totals, heads)
    coming = Scan(False, n_sp, me, c, (bzin, bzout, bmin, bmout), bsem, totals, heads)
    past.clear()
    coming.clear()
    for cp in loads:
        cp.wait()
    swap_tot.wait()

    def compute(k):
        src = peer(k)

        @pl.when(k < 2)
        def _():
            near_pair(k, ocore).wait_recv()

        @pl.when(k >= 2)
        def _():
            near_copy(k, ocore).wait_recv()
            relay_copy(k, ocore).wait_recv()

        pre = 0.0
        act_grad = 0.0
        for t in range(n_tp):
            band = pl.ds(t * q, q)
            spot = full.at[src, t % 2, t // 2]
            pre = pre + dot(spot[0], gu[band, :], 1, 0)
            act_grad = act_grad + dot(spot[1], dw[:, band], 1, 1)
        gate_pre = pre[:, :hid]
        up_pre = pre[:, hid:]
        gate_clip = jnp.minimum(gate_pre, CLAMP_LIMIT)
        up_clip = jnp.clip(up_pre, -CLAMP_LIMIT, CLAMP_LIMIT)
        sig = 1.0 / (1.0 + jnp.exp(-GATE_SLOPE * gate_clip))
        gated = gate_clip * sig
        act[src] = (gated * (up_clip + 1.0)).astype(BF16)
        slope = sig + GATE_SLOPE * gated * (1.0 - sig)
        gpg = jnp.where(gate_pre < CLAMP_LIMIT, act_grad * (up_clip + 1.0) * slope, 0.0)
        upg = jnp.where(jnp.abs(up_pre) < CLAMP_LIMIT, act_grad * gated, 0.0)
        both = jnp.concatenate([gpg, upg], axis=1).astype(BF16)
        gug[src] = both
        for t in range(n_tp):
            back[k, t % 2, t // 2] = dot(both, gu[pl.ds(t * q, q), :], 1, 1).astype(BF16)
        part_copy(k).start()

    def first(k):
        part_copy(k).wait_recv()
        xbuf[k] = (back[k, core, oplane].astype(F32) + part[k, oplane].astype(F32)).astype(BF16)
        x_copy(k).start()

    def second(k):
        x_copy(k).wait_recv()
        total = (
            back[k, core, plane].astype(F32) + part[k, plane].astype(F32) + xrecv[k].astype(F32)
        ).astype(BF16)

        @pl.when(k == 0)
        def _():
            ret[0] = total

        @pl.when(k > 0)
        def _():
            sendbuf[k] = total
            home_copy(k).start()

    def local_retention():
        for h in range(heads):
            score = dot(qr[h], kr[h], 1, 1) * mask[h]
            wts[h] = score.astype(BF16)
            normed_f[:, h * vd : (h + 1) * vd] = dot(
                wts[h], values[:, h * vd : (h + 1) * vd], 1, 0
            )

    def step(n, carry):
        @pl.when(n == 1)
        def _():
            push(pack.at[1], full.at[peer(1), core], ssem.at[1], rsem.at[1], (me, far)).wait_recv()
            near_pair(1, core).start()

        @pl.when((n >= 2) & (n < n_sp))
        def _():
            spot = full.at[peer(n), core, plane]
            push(spot, spot, ssem.at[n], rsem.at[n], (me, far)).wait_recv()
            far_copy(n, plane).start()
            near_copy(n, core).start()

        @pl.when((n >= 3) & (n <= n_sp))
        def _():
            far_copy(n - 1, oplane).wait_recv()
            relay_copy(n - 1, core).start()

        @pl.when(n == past.slot)
        def _():
            past.step(inner)

        @pl.when(n == 1)
        def _():
            local_retention()

        @pl.when((n >= 2) & (n < n_sp + 2))
        def _():
            compute(n - 2)

        @pl.when((n >= 3) & (n < n_sp + 3))
        def _():
            first(n - 3)

        @pl.when((n >= 4) & (n < n_sp + 4))
        def _():
            second(n - 4)

        return carry

    lax.fori_loop(0, n_sp + 4, step, 0)

    for j in range(heads * SPLIT):
        incoming[j // SPLIT, pl.ds((j % SPLIT) * rows_of, rows_of), :] = past.result(j)
    for h in range(heads):
        band = slice(h * vd, (h + 1) * vd)
        kept = normed_f[:, band] + dec[h] * dot(qr[h], incoming[h], 1, 0)
        inverse = lax.rsqrt(jnp.mean(kept * kept, axis=1, keepdims=True) + EPSILON)
        inv[h] = inverse
        normed_f[:, band] = kept * inverse
        normed_own[:, band] = (kept * inverse).astype(BF16)
    normed_all[me] = normed_own[...]
    spread = Chain(normed_own, normed_all, n_sp, me, c, chain_sem, (0, 1))

    def arrive(k, carry):
        push(sendbuf.at[k], ret.at[k], hs.at[k], hr.at[k], (me, far)).wait_recv()
        return carry

    lax.fori_loop(1, n_sp, arrive, 0)

    def combine(k, total):
        return total + dot(pick[peer(k)], ret[k], 0, 0)

    mine = resid.at[core, plane]
    total = lax.fori_loop(0, n_sp, combine, og[:, cols(c)].astype(F32))
    resid[core, plane] = total.astype(BF16)
    to_far = push(mine, mine, gs.at[0], gr.at[0], (me, far))
    to_near = push(mine, mine, gs.at[1], gr.at[1], (me, near))
    to_far.start()
    to_near.start()
    spread.start()
    spot = resid.at[core, oplane]
    push(spot, spot, gs.at[0], gr.at[0], (me, far)).wait_recv()
    onward = push(spot, spot, gs.at[2], gr.at[2], (me, near))
    onward.start()
    for s, p in ((1, plane), (2, oplane)):
        spot = resid.at[ocore, p]
        push(spot, spot, gs.at[s], gr.at[s], (me, near)).wait_recv()

    half = tokens // 2
    group = rcols.shape[3]
    per_quarter = q // group
    per_group = group * n_sp // (q * n_tp)

    def band_of(index):
        g = index // per_group
        quarter = g // per_quarter
        return resid.at[
            lax.rem(quarter, 2), quarter // 2, pl.ds(core * half, half),
            pl.ds(pl.multiple_of(lax.rem(g, per_quarter) * group, 128), group),
        ]

    def col_copy(k):
        return push(band_of(peer(k)), rcols.at[me, core], cs.at[k], cr.at[k], (peer(k), c))

    def col_near(k, side):
        spot = rcols.at[peer(k), side]
        return push(spot, spot, ds.at[k], dr.at[k], (me, near))

    def send_cols(k, carry):
        col_copy(k).start()
        return carry

    lax.fori_loop(1, n_sp, send_cols, 0)
    for side in range(2):
        g = me // per_group
        quarter = g // per_quarter
        rcols[me, side] = resid[
            lax.rem(quarter, 2), quarter // 2, side * half : (side + 1) * half,
            pl.ds(pl.multiple_of(lax.rem(g, per_quarter) * group, 128), group),
        ]
    normed_grad = 0.0
    for t in range(n_tp):
        normed_grad = normed_grad + dot(
            resid[t % 2, t // 2], pw[pl.ds(t * q, q), :], 1, 0
        )
    grads = []
    for h in range(heads):
        band = slice(h * vd, (h + 1) * vd)
        ng = normed_grad[:, band]
        nf = normed_f[:, band]
        grad = inv[h] * (ng - nf * jnp.mean(ng * nf, axis=1, keepdims=True))
        grad_bf = grad.astype(BF16)
        grads.append(grad_bf)
        turned = (qr[h].astype(F32) * dec[h]).astype(BF16)
        state = dot(turned, grad_bf, 0, 0)
        for s in range(SPLIT):
            inner_g[h * SPLIT + s] = state[s * rows_of : (s + 1) * rows_of]

    def weights_grad(t):
        x = flat(full[:, lax.rem(t, 2), t // 2, 0])
        g = flat(full[:, lax.rem(t, 2), t // 2, 1])
        both = dot(x, flat(gug[...]), 0, 0).astype(BF16)
        gout[cols(t), :] = both[:, :hid]
        uout[cols(t), :] = both[:, hid:]
        dout[:, cols(t)] = dot(flat(act[...]), g, 0, 0).astype(BF16)

    def late(s, carry):
        @pl.when(s == coming.slot)
        def _():
            coming.step(inner_g)

        @pl.when(s < n_tp)
        def _():
            weights_grad(s)

        return carry

    lax.fori_loop(0, max(n_sp // 2, n_tp), late, 0)
    stores = [
        pltpu.make_async_copy(gout, gate_o.at[0], osem.at[0]),
        pltpu.make_async_copy(uout, up_o.at[0], osem.at[1]),
        pltpu.make_async_copy(dout, down_o.at[0], osem.at[2]),
    ]
    for cp in stores:
        cp.start()
    for d in range(1, n_sp // 2):
        spread.step(d)

    def relay_cols(k, carry):
        spot = rcols.at[peer(k), core]
        push(spot, spot, cs.at[k], cr.at[k], (me, far)).wait_recv()
        col_near(k, core).start()
        return carry

    lax.fori_loop(1, n_sp, relay_cols, 0)

    def unturn(x):
        return x * cosb[...] - swapped(x) * sinb[...]

    partial = []
    for h in range(heads):
        band = slice(h * vd, (h + 1) * vd)
        score = (dot(grads[h], values[:, band], 1, 1) * mask[h]).astype(BF16)
        qp = dot(score, kr[h], 1, 0) + dec[h] * dot(grads[h], incoming[h], 1, 1)
        query_o[:, h * kd : (h + 1) * kd] = unturn(qp).astype(BF16)
        partial.append((dot(score, qr[h], 0, 0), dot(wts[h], grads[h], 0, 0)))

    def near_cols(k, carry):
        col_near(k, ocore).wait_recv()
        return carry

    lax.fori_loop(1, n_sp, near_cols, 0)
    spread.finish()
    columns = rcols[...].reshape(n_sp * tokens, group)
    everyone = normed_all[...].reshape(n_sp * tokens, heads * vd)
    proj[...] = dot(columns, everyone, 0, 0)
    width = proj_o.shape[0]
    proj_o[...] = proj[pl.ds(pl.multiple_of(lax.rem(me, per_group) * width, 8), width), :]

    future = [coming.result(j) for j in range(heads * SPLIT)]
    for h in range(heads):
        band = slice(h * vd, (h + 1) * vd)
        key_part, value_part = partial[h]
        later = jnp.concatenate(future[h * SPLIT : (h + 1) * SPLIT], axis=0)
        kp = key_part + rem_[h] * dot(values[:, band], later, 1, 1)
        key_o[:, h * kd : (h + 1) * kd] = (unturn(kp) * scale).astype(BF16)
        value_o[:, band] = (value_part + rem_[h] * dot(kr[h], later, 1, 0)).astype(BF16)

    for cp in (to_far, to_near, onward):
        cp.wait_send()
    past.finish()
    coming.finish()

    def drain(k, carry):
        part_copy(k).wait_send()
        x_copy(k).wait_send()

        @pl.when(k < 2)
        def _():
            near_pair(k, core).wait_send()

        @pl.when(k == 1)
        def _():
            out_pair().wait_send()

        @pl.when(k >= 2)
        def _():
            out_copy(k).wait_send()
            far_copy(k, plane).wait_send()
            near_copy(k, core).wait_send()
            relay_copy(k, core).wait_send()

        @pl.when(k > 0)
        def _():
            home_copy(k).wait_send()
            col_copy(k).wait_send()
            col_near(k, core).wait_send()

        return carry

    lax.fori_loop(0, n_sp, drain, 0)
    for cp in stores:
        cp.wait()


def rotation_tables(n_sp, tokens, key_width):
    frequency = 10000.0 ** -np.linspace(0.0, 1.0, key_width // 2)
    frequency = np.repeat(frequency, 2)
    angle = np.arange(tokens)[:, None] * frequency[None, :]
    start = tokens * np.arange(n_sp)[:, None] * frequency[None, :]
    return [
        jnp.asarray(table.astype(np.float32))
        for table in (np.cos(angle), np.sin(angle), np.cos(start), np.sin(start))
    ]


def per_device(
    stream, out_grad, routes, route_weight, queries, key_vectors, value_vectors, log_decay,
    out_proj, gate_weight, up_weight, down_weight,
):
    n_sp = lax.axis_size("sp")
    n_tp = lax.axis_size("tp")
    tokens, width = stream.shape
    cap = 4 * tokens // n_sp
    q = width // n_tp
    heads, kd = queries.shape[1:]
    vd = value_vectors.shape[2]
    hid = gate_weight.shape[2]
    w = width // n_sp
    group = max(w, 128)
    count, rows_of = heads * SPLIT, kd // SPLIT
    vmem, dma = pltpu.VMEM, pltpu.SemaphoreType.DMA
    block = vmem((n_sp, cap, q), BF16)
    packet = vmem((count, rows_of, vd), BF16)
    tables = rotation_tables(n_sp, tokens, kd)
    outs = pl.pallas_call(
        functools.partial(whole_kernel, n_sp, n_tp, heads),
        out_shape=(
            jax.ShapeDtypeStruct(gate_weight.shape, BF16),
            jax.ShapeDtypeStruct(up_weight.shape, BF16),
            jax.ShapeDtypeStruct(down_weight.shape, BF16),
            jax.ShapeDtypeStruct((w, heads * vd), F32),
            jax.ShapeDtypeStruct((tokens, heads * kd), BF16),
            jax.ShapeDtypeStruct((tokens, heads * kd), BF16),
            jax.ShapeDtypeStruct((tokens, heads * vd), BF16),
        ),
        in_specs=vmem_specs(12) + any_specs(4),
        out_specs=tuple(any_specs(3) + vmem_specs(4)),
        scratch_shapes=[
            vmem((n_sp, 2, 2, 2, cap, q), BF16),
            vmem((n_sp, 2, 2, cap, q), BF16),
            vmem((width, 2 * hid), BF16),
            vmem((hid, width), BF16),
            vmem((width, heads * vd), BF16),
            vmem((n_sp, cap, hid), BF16),
            vmem((n_sp, cap, 2 * hid), BF16),
            vmem((n_sp, 2, 2, cap, q), BF16),
            vmem((n_sp, 2, cap, q), BF16),
            block, block, block, block,
            vmem((width, hid), BF16),
            vmem((width, hid), BF16),
            vmem((hid, width), BF16),
            vmem((n_sp, cap, tokens), BF16),
            vmem((n_sp, cap, 1), F32),
            vmem((n_sp, tokens), F32),
            vmem((n_sp, tokens), F32),
            vmem((2, 2, tokens, q), BF16),
            vmem((n_sp, 2, tokens // 2, group), BF16),
            vmem((tokens, heads * vd), BF16),
            vmem((n_sp, tokens, heads * vd), BF16),
            vmem((tokens, heads * vd), F32),
            vmem((heads, tokens, 1), F32),
            vmem((heads, tokens, 1), F32),
            vmem((heads, tokens, 1), F32),
            vmem((heads, tokens, tokens), F32),
            vmem((heads, tokens, tokens), BF16),
            vmem((heads, tokens, kd), BF16),
            vmem((heads, tokens, kd), BF16),
            vmem((tokens, kd), F32),
            vmem((tokens, kd), F32),
            vmem((heads, 8, 128), F32),
            vmem((heads, 8, 128), F32),
            vmem((count, rows_of, vd), F32),
            vmem((count, rows_of, vd), F32),
            vmem((heads, kd, vd), BF16),
            vmem((group, heads * vd), F32),
        ]
        + [packet] * 8
        + [dma((4,)), dma((3,)), dma((2,))]
        + [dma((n_sp,))] * 14
        + [dma((3,))] * 2
        + [dma((n_sp,))] * 4
        + [dma((count,))] * 8
        + [dma((2, n_sp // 2))] * 4,
        compiler_params=pltpu.CompilerParams(
            collective_id=0, has_side_effects=True, vmem_limit_bytes=60 * 2**20
        ),
        name="whole",
    )(
        stream, out_grad, routes.T, route_weight.T, queries.reshape(tokens, heads * kd),
        key_vectors.reshape(tokens, heads * kd), value_vectors.reshape(tokens, heads * vd),
        log_decay, *tables, gate_weight, up_weight, down_weight, out_proj,
    )
    gate, up, down, proj, query, key, value = outs
    return (
        gate, up, down, proj, query.reshape(queries.shape), key.reshape(queries.shape),
        value.reshape(value_vectors.shape),
    )


def solution(mesh):
    in_specs = (
        P("sp", None),
        P("sp", None),
        P("sp", None),
        P("sp", None),
        P("sp", "tp", None),
        P("sp", "tp", None),
        P("sp", "tp", None),
        P("sp", "tp"),
        P(None, "tp"),
        P("sp", None, "tp"),
        P("sp", None, "tp"),
        P("sp", "tp", None),
    )
    out_specs = (
        P("sp", None, "tp"),
        P("sp", None, "tp"),
        P("sp", "tp", None),
        P("sp", "tp"),
        P("sp", "tp", None),
        P("sp", "tp", None),
        P("sp", "tp", None),
    )
    return jax.shard_map(
        per_device, mesh=mesh, in_specs=in_specs, out_specs=out_specs, check_vma=False
    )
```

time: 155 us -> 119 us (0.77)
  matrix products: 12.5 us -> 0 us
  Pallas kernels: 116 us -> 104 us
  other arithmetic: 8.88 us -> 0 us
    dot_general x21 -> x0, matrix products: 12.5 us -> none  [the longest x1 2.78 us: mm(): lax.dot_general(a, b, (((da,), (db,)), ((), ())), preferred_element_type=...]
    pallas_call x2 -> x1, Pallas kernels: 116 us -> 104 us  [per_device(): pl.pallas_call(functools.partial(whole_kernel, n_sp, n_tp, heads), out_sh...]
    reshape x1 -> x4, local copies, waits for them, and re-layouts: 1.08 us -> 6.19 us  [the longest x1 1.59 us: per_device(): value.reshape(value_vectors.shape)]
    reduce_sum x7 -> x0, other arithmetic: 3.84 us -> none  [the longest x2 1.99 us: weighted(): return jnp.sum(kept * factors[:, :, None, None], axis=0)]
    unnamed x61 -> x12, local copies, waits for them, and re-layouts: 7.93 us -> 8.08 us
where the time goes in v2:
time: 119 us
  Pallas kernels  104 us (87%)
  local copies, waits for them, and re-layouts  14.3 us (12%)
    pallas_call x1, Pallas kernels, per_device(): pl.pallas_call(functools.partial(whole_kernel, n_sp, n_tp, heads), out_sh...  104 us
    unnamed x12, local copies, waits for them, and re-layouts  8.08 us

profile of v2, /device:TPU:0, one launch (start us, length us, event | category | flops | bytes accessed | tf_op | source)
XLA Modules:
  0.0 118.7 jit_solution(14246694103211274149)
XLA Ops:
  0.6 1.4 %copy.23.log_decay = f32[128,2]{1,0:T(8,128)} copy(f32[128,2]{0,1:T(2,128)} %param.23) | data formatting | bytes 2048 | tf_op args[7]
  2.0 1.6 %copy.26 = bf16[16,8,2,256]{3,1,2,0:T(8,128)(2,1)} copy(bf16[16,8,2,256]{3,2,1,0:T(2,128)(2,1)} %bitcast.11) | data formatting | bytes 262144
  3.6 1.5 %copy_bitcast_fusion = (bf16[128,256]{1,0:T(8,128)(2,1)}, bf16[128,256]{1,0:T(8,128)(2,1)}) fusion(bf16[16,8,2,128]{3,2,1,0:T(2,128)(2,1)} %bitcast.12, bf16[16,8,2,128]{3,2,1,0:T(2,128)(2,1)} %bitcast.13), kind=kLoop, calls=%fused_computation | loop fusion | bytes 262144 | tf_op jit(solution)/shard_map/reshape | solution.py:771
  5.2 103.8 %whole.1 = (bf16[1,2048,256]{2,1,0:T(8,128)(2,1)}, bf16[1,2048,256]{2,1,0:T(8,128)(2,1)}, bf16[1,256,2048]{2,1,0:T(8,128)(2,1)}, f32[256,512]{1,0:T(8,128)}, bf1...) custom-call(bf16[128,2048]{1,0:T(8,128)(2,1)} %stream.1, bf16[128,2048]{1,0:T(8,128)(2,1)} %og.1, ...), custom_call_target="tpu_custom_call" | custom-call | tf_op jit(solution)/shard_map/whole/pallas_call | solution.py:706
  108.9 0.0 copy-start.1
  108.9 1.6 %reshape.35 = bf16[128,2,128]{2,1,0:T(2,128)(2,1)} reshape(bf16[128,256]{1,0:T(8,128)(2,1)} %get-tuple-element.18) | data formatting | bytes 131072 | tf_op jit(solution)/shard_map/reshape | solution.py:776
  110.5 1.5 %reshape.36 = bf16[128,2,128]{2,1,0:T(2,128)(2,1)} reshape(bf16[128,256]{1,0:T(8,128)(2,1)} %get-tuple-element.19) | data formatting | bytes 131072 | tf_op jit(solution)/shard_map/reshape | solution.py:776
  112.0 1.6 %reshape.37 = bf16[128,2,256]{2,1,0:T(2,128)(2,1)} reshape(bf16[128,512]{1,0:T(8,128)(2,1)} %get-tuple-element.20) | data formatting | bytes 262144 | tf_op jit(solution)/shard_map/reshape | solution.py:777
  113.6 0.0 copy-start
  113.6 2.4 %copy.33 = bf16[1,2048,256]{2,1,0:T(8,128)(2,1)} copy(bf16[1,2048,256]{2,1,0:T(8,128)(2,1)} %get-tuple-element.30) | data formatting | bytes 2097152
  115.9 0.0 copy-done.1
  116.0 0.0 copy-start.2
  116.0 1.0 copy.34
  116.9 0.0 copy-done
  116.9 1.0 copy.35
  117.9 0.0 copy-done.2
  117.9 0.8 copy.36
Async XLA Ops:
  108.9 7.0 %copy-start.1 = (bf16[1,2048,256]{2,1,0:T(8,128)(2,1)S(1)}, bf16[1,2048,256]{2,1,0:T(8,128)(2,1)}, u32[]{:S(2)}) copy-start(bf16[1,2048,256]{2,1,0:T(8,128)(2,1)} %get-tuple-element.31) | copy-start | bytes 3145732
  113.6 3.3 %copy-start = (bf16[1,256,2048]{2,1,0:T(8,128)(2,1)S(1)}, bf16[1,256,2048]{2,1,0:T(8,128)(2,1)}, u32[]{:S(2)}) copy-start(bf16[1,256,2048]{2,1,0:T(8,128)(2,1)} %get-tuple-element.32) | copy-start | bytes 3145732
  116.0 1.9 %copy-start.2 = (f32[256,512]{1,0:T(8,128)S(1)}, f32[256,512]{1,0:T(8,128)}, u32[]{:S(2)}) copy-start(f32[256,512]{1,0:T(8,128)} %get-tuple-element.33) | copy-start | bytes 1572868

commit v3 on v2

--- a/solution.py
+++ b/solution.py
@@ -207,11 +207,11 @@
     stream, og, routes, route_w, queries, keys, values, log_decay, cos_t, sin_t, cos_s, sin_s,
     gate_w, up_w, down_w, proj_w,
     gate_o, up_o, down_o, proj_o, query_o, key_o, value_o,
-    full, pack, gu, dw, pw, act, gug, back, part, xbuf, xrecv, sendbuf, ret, gout, uout, dout,
+    full, pack, gu, dw, pw, act, gug, back, part, xbuf, xrecv, sendbuf, ret,
     pick, wcol, slotmap, weight_map, resid, rcols, normed_own, normed_all, normed_f, inv, dec, rem_,
-    mask, wts, qr, kr, cosb, sinb, totb, toto, inner, inner_g, incoming, proj,
+    mask, wts, qr, kr, val, cosb, sinb, totb, toto, inner, inner_g, incoming, proj,
     fzin, fzout, fmin, fmout, bzin, bzout, bmin, bmout,
-    wsem, osem, tsem, ssem, rsem, fs, fr, ns, nr, es, er, ps, pr, xs, xr, hs, hr, gs, gr,
+    wsem, tsem, ssem, rsem, fs, fr, ns, nr, es, er, ps, pr, xs, xr, hs, hr, gs, gr,
     cs, cr, ds, dr, *more,
 ):
     fsem, bsem, chain_sem = more[0:4], more[4:8], more[8:12]
@@ -226,7 +226,7 @@
     hid = dw.shape[0]
     tokens = stream.shape[0]
     kd = cos_t.shape[1]
-    vd = values.shape[1] // heads
+    vd = values.shape[2]
     scale = kd ** (-0.5)
     bits = [1 << b for b in range((n_sp - 1).bit_length())]
 
@@ -317,62 +317,71 @@
     fill(pack.at[1, plane], peer(1), c)
     fill(pack.at[1, oplane], peer(1), far)
     fill(pack.at[2, plane], peer(2), c)
-    pl.semaphore_wait(barrier, n_sp - 1 + 2)
-    out_pair().start()
-
-    def send_out(k, carry):
-        @pl.when(k < n_sp)
-        def _():
-            fill(pack.at[k, plane], peer(k), c)
-
-        out_copy(k - 1).start()
-        return carry
-
-    lax.fori_loop(3, n_sp + 1, send_out, 0)
-    fill(full.at[me, core, plane], me, c)
-    fill(full.at[me, core, oplane], me, far)
-
-    lower = jnp.where(row >= col, 1.0, 0.0)
     running = lax.dot_general(
-        lower, log_decay[...], (((1,), (0,)), ((), ())), preferred_element_type=F32,
-        precision=lax.Precision.HIGHEST,
+        log_decay[...], jnp.where(row <= col, 1.0, 0.0), (((1,), (0,)), ((), ())),
+        preferred_element_type=F32, precision=lax.Precision.HIGHEST,
     )
     for h in range(heads):
-        totb[h] = jnp.broadcast_to(running[tokens - 1 : tokens, h : h + 1], totb.shape[1:])
-    near_pair(0, core).start()
+        totb[h] = jnp.broadcast_to(running[h : h + 1, tokens - 1 : tokens], totb.shape[1:])
     start_cos, start_sin = cos_s[pl.ds(me, 1), :], sin_s[pl.ds(me, 1), :]
     cosines = start_cos * cos_t[...] - start_sin * sin_t[...]
     sines = start_sin * cos_t[...] + start_cos * sin_t[...]
     cosb[...] = cosines
     sinb[...] = sines
-    swap_tot = push(totb, toto, tsem.at[0], tsem.at[1], (other, c))
-    swap_tot.start()
     rows_of = kd // SPLIT
     for h in range(heads):
-        x = queries[:, h * kd : (h + 1) * kd].astype(F32)
+        x = queries[:, h, :].astype(F32)
         qr[h] = (x * cosines + swapped(x) * sines).astype(BF16)
-        x = keys[:, h * kd : (h + 1) * kd].astype(F32)
+        x = keys[:, h, :].astype(F32)
         key = (x * cosines + swapped(x) * sines) * scale
         kr[h] = key.astype(BF16)
-        run = running[:, h : h + 1]
-        left = jnp.exp(running[tokens - 1 : tokens, h : h + 1] - run)
+        val[h] = values[:, h, :]
+        along = jnp.broadcast_to(running[h : h + 1, :], (tokens, tokens))
+        down = along.T
+        run = down[:, 0:1]
+        left = jnp.exp(running[h : h + 1, tokens - 1 : tokens] - run)
         dec[h] = jnp.exp(run)
         rem_[h] = left
-        state = dot((key * left).astype(BF16), values[:, h * vd : (h + 1) * vd], 0, 0)
+        state = dot((key * left).astype(BF16), val[h], 0, 0)
         for s in range(SPLIT):
             inner[h * SPLIT + s] = state[s * rows_of : (s + 1) * rows_of]
-        spread_run = jnp.broadcast_to(run, (tokens, tokens))
-        difference = spread_run - spread_run.T
         causal = row >= col
-        mask[h] = jnp.where(causal, jnp.exp(jnp.where(causal, difference, 0.0)), 0.0)
+        mask[h] = jnp.where(causal, jnp.exp(jnp.where(causal, down - along, 0.0)), 0.0)
     totals = (totb, toto)
     past = Scan(True, n_sp, me, c, (fzin, fzout, fmin, fmout), fsem, totals, heads)
     coming = Scan(False, n_sp, me, c, (bzin, bzout, bmin, bmout), bsem, totals, heads)
     past.clear()
     coming.clear()
+    pairs = n_sp // 2
+    pace = (n_sp + 4) // pairs
+    early = n_sp * 3 // 4
+    pl.semaphore_wait(barrier, n_sp - 1 + 2)
+    swap_tot = push(totb, toto, tsem.at[0], tsem.at[1], (other, c))
+    swap_tot.start()
+    out_pair().start()
+    out_copy(2).start()
+    fill(full.at[me, core, plane], me, c)
+    fill(full.at[me, core, oplane], me, far)
+
+    def fill_rest(k, carry):
+        fill(pack.at[k, plane], peer(k), c)
+        return carry
+
+    lax.fori_loop(3, n_sp, fill_rest, 0)
+    near_pair(0, core).start()
+    swap_tot.wait()
+
+    @pl.when(past.slot == 0)
+    def _():
+        past.step(inner)
+
+    def send_out(k, carry):
+        out_copy(k).start()
+        return carry
+
+    lax.fori_loop(3, early, send_out, 0)
     for cp in loads:
         cp.wait()
-    swap_tot.wait()
 
     def compute(k):
         src = peer(k)
@@ -433,51 +442,68 @@
         for h in range(heads):
             score = dot(qr[h], kr[h], 1, 1) * mask[h]
             wts[h] = score.astype(BF16)
-            normed_f[:, h * vd : (h + 1) * vd] = dot(
-                wts[h], values[:, h * vd : (h + 1) * vd], 1, 0
-            )
+            normed_f[:, h * vd : (h + 1) * vd] = dot(wts[h], val[h], 1, 0)
+
+    def turn_of(n):
+        return jnp.where((n >= 1) & (n <= 4), 1 + lax.rem(n, 4), n)
+
+    compute(0)
+    local_retention()
 
     def step(n, carry):
+        k = turn_of(n)
+
+        @pl.when((n < n_sp) & (k == 1))
+        def _():
+            spot = full.at[peer(1), core]
+            push(spot, spot, ssem.at[1], rsem.at[1], (me, far)).wait_recv()
+            near_pair(1, core).start()
+
+        @pl.when((n < n_sp) & (k > 1))
+        def _():
+            spot = full.at[peer(k), core, plane]
+            push(spot, spot, ssem.at[k], rsem.at[k], (me, far)).wait_recv()
+            far_copy(k, plane).start()
+            near_copy(k, core).start()
+
+        j = turn_of(n - 1)
+
+        @pl.when((n <= n_sp) & (j > 1))
+        def _():
+            far_copy(j, oplane).wait_recv()
+            relay_copy(j, core).start()
+
+        @pl.when((n == past.slot * pace) & (past.slot > 0))
+        def _():
+            past.step(inner)
+
+        @pl.when(n == pace)
+        def _():
+            lax.fori_loop(early, n_sp, send_out, 0)
+
         @pl.when(n == 1)
         def _():
-            push(pack.at[1], full.at[peer(1), core], ssem.at[1], rsem.at[1], (me, far)).wait_recv()
-            near_pair(1, core).start()
-
-        @pl.when((n >= 2) & (n < n_sp))
-        def _():
-            spot = full.at[peer(n), core, plane]
-            push(spot, spot, ssem.at[n], rsem.at[n], (me, far)).wait_recv()
-            far_copy(n, plane).start()
-            near_copy(n, core).start()
-
-        @pl.when((n >= 3) & (n <= n_sp))
-        def _():
-            far_copy(n - 1, oplane).wait_recv()
-            relay_copy(n - 1, core).start()
-
-        @pl.when(n == past.slot)
-        def _():
-            past.step(inner)
-
-        @pl.when(n == 1)
-        def _():
-            local_retention()
-
-        @pl.when((n >= 2) & (n < n_sp + 2))
-        def _():
-            compute(n - 2)
-
-        @pl.when((n >= 3) & (n < n_sp + 3))
-        def _():
-            first(n - 3)
-
-        @pl.when((n >= 4) & (n < n_sp + 4))
-        def _():
-            second(n - 4)
+            first(0)
+
+        @pl.when(n == 2)
+        def _():
+            second(0)
+
+        @pl.when((n >= 3) & (n < n_sp + 2))
+        def _():
+            compute(turn_of(n - 2))
+
+        @pl.when((n >= 4) & (n < n_sp + 3))
+        def _():
+            first(turn_of(n - 3))
+
+        @pl.when((n >= 5) & (n < n_sp + 4))
+        def _():
+            second(turn_of(n - 4))
 
         return carry
 
-    lax.fori_loop(0, n_sp + 4, step, 0)
+    lax.fori_loop(1, n_sp + 4, step, 0)
 
     for j in range(heads * SPLIT):
         incoming[j // SPLIT, pl.ds((j % SPLIT) * rows_of, rows_of), :] = past.result(j)
@@ -490,33 +516,48 @@
         normed_own[:, band] = (kept * inverse).astype(BF16)
     normed_all[me] = normed_own[...]
     spread = Chain(normed_own, normed_all, n_sp, me, c, chain_sem, (0, 1))
-
-    def arrive(k, carry):
+    spread.start()
+
+    def arrive(k, total):
         push(sendbuf.at[k], ret.at[k], hs.at[k], hr.at[k], (me, far)).wait_recv()
-        return carry
-
-    lax.fori_loop(1, n_sp, arrive, 0)
-
-    def combine(k, total):
         return total + dot(pick[peer(k)], ret[k], 0, 0)
 
-    mine = resid.at[core, plane]
-    total = lax.fori_loop(0, n_sp, combine, og[:, cols(c)].astype(F32))
+    total = og[:, cols(c)].astype(F32) + dot(pick[me], ret[0], 0, 0)
+    total = lax.fori_loop(1, n_sp, arrive, total)
+    half = tokens // 2
     resid[core, plane] = total.astype(BF16)
-    to_far = push(mine, mine, gs.at[0], gr.at[0], (me, far))
-    to_near = push(mine, mine, gs.at[1], gr.at[1], (me, near))
-    to_far.start()
-    to_near.start()
-    spread.start()
-    spot = resid.at[core, oplane]
-    push(spot, spot, gs.at[0], gr.at[0], (me, far)).wait_recv()
-    onward = push(spot, spot, gs.at[2], gr.at[2], (me, near))
-    onward.start()
-    for s, p in ((1, plane), (2, oplane)):
-        spot = resid.at[ocore, p]
-        push(spot, spot, gs.at[s], gr.at[s], (me, near)).wait_recv()
-
-    half = tokens // 2
+
+    def strip(side, p, i):
+        return resid.at[side, p, pl.ds(i * half, half)]
+
+    sent = []
+    for i in range(2):
+        mine = strip(core, plane, i)
+        sent.append(push(mine, mine, gs.at[0, i], gr.at[0, i], (me, far)))
+    for i in range(2):
+        mine = strip(core, plane, i)
+        sent.append(push(mine, mine, gs.at[1, i], gr.at[1, i], (me, near)))
+    for cp in sent:
+        cp.start()
+    spread.step(1)
+
+    def share(side, p):
+        return dot(resid[side, p], pw[cols(2 * p + side), :], 1, 0)
+
+    normed_grad = share(core, plane)
+    for i in range(2):
+        spot = strip(core, oplane, i)
+        push(spot, spot, gs.at[0, i], gr.at[0, i], (me, far)).wait_recv()
+        onward = push(spot, spot, gs.at[2, i], gr.at[2, i], (me, near))
+        onward.start()
+        sent.append(onward)
+    normed_grad = normed_grad + share(core, oplane)
+    for j, p in ((1, plane), (2, oplane)):
+        for i in range(2):
+            spot = strip(ocore, p, i)
+            push(spot, spot, gs.at[j, i], gr.at[j, i], (me, near)).wait_recv()
+        normed_grad = normed_grad + share(ocore, p)
+
     group = rcols.shape[3]
     per_quarter = q // group
     per_group = group * n_sp // (q * n_tp)
@@ -540,19 +581,6 @@
         col_copy(k).start()
         return carry
 
-    lax.fori_loop(1, n_sp, send_cols, 0)
-    for side in range(2):
-        g = me // per_group
-        quarter = g // per_quarter
-        rcols[me, side] = resid[
-            lax.rem(quarter, 2), quarter // 2, side * half : (side + 1) * half,
-            pl.ds(pl.multiple_of(lax.rem(g, per_quarter) * group, 128), group),
-        ]
-    normed_grad = 0.0
-    for t in range(n_tp):
-        normed_grad = normed_grad + dot(
-            resid[t % 2, t // 2], pw[pl.ds(t * q, q), :], 1, 0
-        )
     grads = []
     for h in range(heads):
         band = slice(h * vd, (h + 1) * vd)
@@ -570,31 +598,43 @@
         x = flat(full[:, lax.rem(t, 2), t // 2, 0])
         g = flat(full[:, lax.rem(t, 2), t // 2, 1])
         both = dot(x, flat(gug[...]), 0, 0).astype(BF16)
-        gout[cols(t), :] = both[:, :hid]
-        uout[cols(t), :] = both[:, hid:]
-        dout[:, cols(t)] = dot(flat(act[...]), g, 0, 0).astype(BF16)
+        gate_o[0, cols(t), :] = both[:, :hid]
+        up_o[0, cols(t), :] = both[:, hid:]
+        down_o[0, :, cols(t)] = dot(flat(act[...]), g, 0, 0).astype(BF16)
+
+    @pl.when(coming.slot == 0)
+    def _():
+        coming.step(inner_g)
+
+    lax.fori_loop(1, n_sp, send_cols, 0)
 
     def late(s, carry):
-        @pl.when(s == coming.slot)
+        @pl.when((s == coming.slot) & (s > 0))
         def _():
             coming.step(inner_g)
 
+        if pairs > 2:
+
+            @pl.when(s == 1)
+            def _():
+                spread.step(2)
+
         @pl.when(s < n_tp)
         def _():
             weights_grad(s)
 
         return carry
 
-    lax.fori_loop(0, max(n_sp // 2, n_tp), late, 0)
-    stores = [
-        pltpu.make_async_copy(gout, gate_o.at[0], osem.at[0]),
-        pltpu.make_async_copy(uout, up_o.at[0], osem.at[1]),
-        pltpu.make_async_copy(dout, down_o.at[0], osem.at[2]),
-    ]
-    for cp in stores:
-        cp.start()
-    for d in range(1, n_sp // 2):
+    lax.fori_loop(0, max(pairs, n_tp), late, 0)
+    for d in range(3, pairs):
         spread.step(d)
+    for side in range(2):
+        g = me // per_group
+        quarter = g // per_quarter
+        rcols[me, side] = resid[
+            lax.rem(quarter, 2), quarter // 2, side * half : (side + 1) * half,
+            pl.ds(pl.multiple_of(lax.rem(g, per_quarter) * group, 128), group),
+        ]
 
     def relay_cols(k, carry):
         spot = rcols.at[peer(k), core]
@@ -609,8 +649,7 @@
 
     partial = []
     for h in range(heads):
-        band = slice(h * vd, (h + 1) * vd)
-        score = (dot(grads[h], values[:, band], 1, 1) * mask[h]).astype(BF16)
+        score = (dot(grads[h], val[h], 1, 1) * mask[h]).astype(BF16)
         qp = dot(score, kr[h], 1, 0) + dec[h] * dot(grads[h], incoming[h], 1, 1)
         query_o[:, h * kd : (h + 1) * kd] = unturn(qp).astype(BF16)
         partial.append((dot(score, qr[h], 0, 0), dot(wts[h], grads[h], 0, 0)))
@@ -632,11 +671,11 @@
         band = slice(h * vd, (h + 1) * vd)
         key_part, value_part = partial[h]
         later = jnp.concatenate(future[h * SPLIT : (h + 1) * SPLIT], axis=0)
-        kp = key_part + rem_[h] * dot(values[:, band], later, 1, 1)
+        kp = key_part + rem_[h] * dot(val[h], later, 1, 1)
         key_o[:, h * kd : (h + 1) * kd] = (unturn(kp) * scale).astype(BF16)
         value_o[:, band] = (value_part + rem_[h] * dot(kr[h], later, 1, 0)).astype(BF16)
 
-    for cp in (to_far, to_near, onward):
+    for cp in sent:
         cp.wait_send()
     past.finish()
     coming.finish()
@@ -669,6 +708,20 @@
         return carry
 
     lax.fori_loop(0, n_sp, drain, 0)
+
+
+def finish_kernel(
+    gate, up, down, proj, query, key, value, gate_o, up_o, down_o, proj_o, query_o, key_o, value_o,
+    sem,
+):
+    pairs = ((gate, gate_o), (up, up_o), (down, down_o), (proj, proj_o))
+    stores = [pltpu.make_async_copy(a, b, sem.at[i]) for i, (a, b) in enumerate(pairs)]
+    for cp in stores:
+        cp.start()
+    for a, b in ((query, query_o), (key, key_o), (value, value_o)):
+        width = b.shape[2]
+        for h in range(b.shape[1]):
+            b[:, h, :] = a[:, h * width : (h + 1) * width]
     for cp in stores:
         cp.wait()
 
@@ -714,8 +767,8 @@
             jax.ShapeDtypeStruct((tokens, heads * kd), BF16),
             jax.ShapeDtypeStruct((tokens, heads * vd), BF16),
         ),
-        in_specs=vmem_specs(12) + any_specs(4),
-        out_specs=tuple(any_specs(3) + vmem_specs(4)),
+        in_specs=vmem_specs(12) + [pl.BlockSpec(memory_space=pltpu.HBM)] * 4,
+        out_specs=tuple(vmem_specs(7)),
         scratch_shapes=[
             vmem((n_sp, 2, 2, 2, cap, q), BF16),
             vmem((n_sp, 2, 2, cap, q), BF16),
@@ -727,9 +780,6 @@
             vmem((n_sp, 2, 2, cap, q), BF16),
             vmem((n_sp, 2, cap, q), BF16),
             block, block, block, block,
-            vmem((width, hid), BF16),
-            vmem((width, hid), BF16),
-            vmem((hid, width), BF16),
             vmem((n_sp, cap, tokens), BF16),
             vmem((n_sp, cap, 1), F32),
             vmem((n_sp, tokens), F32),
@@ -746,6 +796,7 @@
             vmem((heads, tokens, tokens), BF16),
             vmem((heads, tokens, kd), BF16),
             vmem((heads, tokens, kd), BF16),
+            vmem((heads, tokens, vd), BF16),
             vmem((tokens, kd), F32),
             vmem((tokens, kd), F32),
             vmem((heads, 8, 128), F32),
@@ -756,26 +807,32 @@
             vmem((group, heads * vd), F32),
         ]
         + [packet] * 8
-        + [dma((4,)), dma((3,)), dma((2,))]
+        + [dma((4,)), dma((2,))]
         + [dma((n_sp,))] * 14
-        + [dma((3,))] * 2
+        + [dma((3, 2))] * 2
         + [dma((n_sp,))] * 4
         + [dma((count,))] * 8
         + [dma((2, n_sp // 2))] * 4,
         compiler_params=pltpu.CompilerParams(
-            collective_id=0, has_side_effects=True, vmem_limit_bytes=60 * 2**20
+            collective_id=0, has_side_effects=True, vmem_limit_bytes=48 * 2**20
         ),
         name="whole",
     )(
-        stream, out_grad, routes.T, route_weight.T, queries.reshape(tokens, heads * kd),
-        key_vectors.reshape(tokens, heads * kd), value_vectors.reshape(tokens, heads * vd),
-        log_decay, *tables, gate_weight, up_weight, down_weight, out_proj,
+        stream, out_grad, routes.T, route_weight.T, queries, key_vectors, value_vectors,
+        log_decay.T, *tables, gate_weight, up_weight, down_weight, out_proj,
     )
-    gate, up, down, proj, query, key, value = outs
-    return (
-        gate, up, down, proj, query.reshape(queries.shape), key.reshape(queries.shape),
-        value.reshape(value_vectors.shape),
-    )
+    shapes = [jax.ShapeDtypeStruct(x.shape, x.dtype) for x in outs[:4]] + [
+        jax.ShapeDtypeStruct(x.shape, BF16) for x in (queries, key_vectors, value_vectors)
+    ]
+    return pl.pallas_call(
+        finish_kernel,
+        out_shape=tuple(shapes),
+        in_specs=vmem_specs(7),
+        out_specs=tuple(any_specs(4) + vmem_specs(3)),
+        scratch_shapes=[dma((4,))],
+        compiler_params=pltpu.CompilerParams(vmem_limit_bytes=16 * 2**20),
+        name="finish",
+    )(*outs)
 
 
 def solution(mesh):

time: 119 us -> 98.8 us (0.83)
  Pallas kernels: 104 us -> 87.9 us
  local copies, waits for them, and re-layouts: 14.3 us -> 9.74 us
    pallas_call x1, Pallas kernels: 104 us -> 85.3 us  [per_device(): pl.pallas_call(functools.partial(whole_kernel, n_sp, n_tp, heads), out_sh...]
    reshape x4 -> x0, local copies, waits for them, and re-layouts: 6.19 us -> none  [the longest x1 1.59 us: per_device(): value.reshape(value_vectors.shape)]
    pallas_call x0 -> x1, Pallas kernels: none -> 2.56 us  [per_device(): pl.pallas_call(finish_kernel, out_shape=tuple(shapes), in_specs=vmem_spec...]
    unnamed x12 -> x24, local copies, waits for them, and re-layouts: 8.08 us -> 9.74 us
where the time goes in v3:
time: 98.8 us; the launch traced here: 98.3 us
  Pallas kernels  87.9 us (89%)
  local copies, waits for them, and re-layouts  9.74 us (10%)
    pallas_call x1, Pallas kernels, per_device(): pl.pallas_call(functools.partial(whole_kernel, n_sp, n_tp, heads), out_sh...  85.3 us
    unnamed x24, local copies, waits for them, and re-layouts  9.74 us
    pallas_call x1, Pallas kernels, per_device(): pl.pallas_call(finish_kernel, out_shape=tuple(shapes), in_specs=vmem_spec...  2.56 us

profile of v3, /device:TPU:0, one launch (start us, length us, event | category | flops | bytes accessed | tf_op | source)
XLA Modules:
  0.0 98.3 jit_solution(14049210877570857251)
XLA Ops:
  0.6 0.0 copy-start
  0.6 1.0 %copy-done = bf16[128,2048]{1,0:T(8,128)(2,1)S(1)} copy-done((bf16[128,2048]{1,0:T(8,128)(2,1)S(1)}, bf16[128,2048]{1,0:T(8,128)(2,1)}, u32[]{:S(2)}) %copy-start) | copy-done | bytes 524312
  1.7 0.0 copy-start.1
  1.7 1.0 %copy-done.1 = bf16[128,2048]{1,0:T(8,128)(2,1)S(1)} copy-done((bf16[128,2048]{1,0:T(8,128)(2,1)S(1)}, bf16[128,2048]{1,0:T(8,128)(2,1)}, u32[]{:S(2)}) %copy-start.1) | copy-done | bytes 524312
  2.7 0.0 copy-start.2
  2.7 0.9 copy-done.2
  3.6 0.0 copy-start.3
  3.6 0.8 copy-done.3
  4.5 0.0 copy-start.4
  4.5 0.8 copy-done.4
  5.3 0.0 copy-start.5
  5.3 0.8 copy-done.5
  6.1 0.0 copy-start.6
  6.1 0.8 copy-done.6
  7.0 0.0 copy-start.7
  7.0 0.7 copy-done.7
  7.7 0.0 copy-start.8
  7.7 0.7 copy-done.8
  8.4 0.0 copy-start.9
  8.4 0.7 copy-done.9
  9.0 0.0 copy-start.10
  9.0 0.7 copy-done.10
  9.7 0.0 copy-start.11
  9.7 0.7 copy-done.11
  10.4 85.3 %whole.1 = (bf16[1,2048,256]{2,1,0:T(8,128)(2,1)S(1)}, bf16[1,2048,256]{2,1,0:T(8,128)(2,1)S(1)}, bf16[1,256,2048]{2,1,0:T(8,128)(2,1)S(1)}, f32[256,512]{1,0:T(...) custom-call(bf16[128,2048]{1,0:T(8,128)(2,1)S(1)} %copy-done, ...), custom_call_target="tpu_custom_call" | custom-call | tf_op jit(solution)/shard_map/whole/pallas_call | solution.py:759
  95.8 2.6 %finish.1 = (bf16[1,2048,256]{2,1,0:T(8,128)(2,1)}, bf16[1,2048,256]{2,1,0:T(8,128)(2,1)}, bf16[1,256,2048]{2,1,0:T(8,128)(2,1)}, f32[256,512]{1,0:T(8,128)}, bf...) custom-call(bf16[1,2048,256]{2,1,0:T(8,128)(2,1)S(1)} %get-tuple-element.14.gate, ...), custom_call_target="tpu_custom_call" | custom-call | tf_op jit(solution)/shard_map/finish/pallas_call | solution.py:827
Async XLA Ops:
  0.6 1.0 %copy-start = (bf16[128,2048]{1,0:T(8,128)(2,1)S(1)}, bf16[128,2048]{1,0:T(8,128)(2,1)}, u32[]{:S(2)}) copy-start(bf16[128,2048]{1,0:T(8,128)(2,1)} %stream.1) | copy-start | bytes 1572868
  1.7 1.0 %copy-start.1 = (bf16[128,2048]{1,0:T(8,128)(2,1)S(1)}, bf16[128,2048]{1,0:T(8,128)(2,1)}, u32[]{:S(2)}) copy-start(bf16[128,2048]{1,0:T(8,128)(2,1)} %og.1) | copy-start | bytes 1572868
  2.7 0.9 copy-start.2
  3.6 0.8 copy-start.3
  4.5 0.8 copy-start.4
  5.3 0.8 copy-start.5
  6.1 0.8 copy-start.6
  7.0 0.7 copy-start.7
  7.7 0.7 copy-start.8
  8.4 0.7 copy-start.9
  9.0 0.7 copy-start.10
  9.7 0.7 copy-start.11

commit v4 on v3

--- a/solution.py
+++ b/solution.py
@@ -281,13 +281,36 @@
         spot[0] = rows.astype(BF16)
         spot[1] = grads.astype(BF16)
 
+    half_sp = n_sp // 2
+
+    def turn_of(n):
+        return n // 2 + lax.rem(n, 2) * half_sp
+
+    def direct(k, act):
+        @pl.when(k < half_sp)
+        def _():
+            act()
+
+    def crossing(k, act):
+        @pl.when(k >= half_sp)
+        def _():
+            act()
+
     def out_copy(k):
         return push(
             pack.at[k, plane], full.at[me, core, plane], ssem.at[k], rsem.at[k], (peer(k), c)
         )
 
-    def out_pair():
-        return push(pack.at[1], full.at[me, core], ssem.at[1], rsem.at[1], (peer(1), c))
+    def out_pair(k):
+        return push(pack.at[k], full.at[me, core], ssem.at[k], rsem.at[k], (peer(k), c))
+
+    def send_out(k):
+        direct(k, lambda: out_pair(k).start())
+        crossing(k, lambda: out_copy(k).start())
+
+    def fill_out(k):
+        fill(pack.at[k, plane], peer(k), c)
+        direct(k, lambda: fill(pack.at[k, oplane], peer(k), far))
 
     def far_copy(k, p):
         spot = full.at[peer(k), core, p]
@@ -314,9 +337,8 @@
     def home_copy(k):
         return push(sendbuf.at[k], ret.at[k], hs.at[k], hr.at[k], (peer(k), c))
 
-    fill(pack.at[1, plane], peer(1), c)
-    fill(pack.at[1, oplane], peer(1), far)
-    fill(pack.at[2, plane], peer(2), c)
+    fill(pack.at[half_sp, plane], peer(half_sp), c)
+    fill_out(1)
     running = lax.dot_general(
         log_decay[...], jnp.where(row <= col, 1.0, 0.0), (((1,), (0,)), ((), ())),
         preferred_element_type=F32, precision=lax.Precision.HIGHEST,
@@ -358,39 +380,39 @@
     pl.semaphore_wait(barrier, n_sp - 1 + 2)
     swap_tot = push(totb, toto, tsem.at[0], tsem.at[1], (other, c))
     swap_tot.start()
-    out_pair().start()
-    out_copy(2).start()
+    out_copy(half_sp).start()
+    out_pair(1).start()
     fill(full.at[me, core, plane], me, c)
     fill(full.at[me, core, oplane], me, far)
-
-    def fill_rest(k, carry):
-        fill(pack.at[k, plane], peer(k), c)
+    near_pair(0, core).start()
+
+    def fill_rest(n, carry):
+        fill_out(turn_of(n))
         return carry
 
+    def send_rest(n, carry):
+        send_out(turn_of(n))
+        return carry
+
     lax.fori_loop(3, n_sp, fill_rest, 0)
-    near_pair(0, core).start()
     swap_tot.wait()
 
     @pl.when(past.slot == 0)
     def _():
         past.step(inner)
 
-    def send_out(k, carry):
-        out_copy(k).start()
-        return carry
-
-    lax.fori_loop(3, early, send_out, 0)
+    lax.fori_loop(3, early, send_rest, 0)
     for cp in loads:
         cp.wait()
 
     def compute(k):
         src = peer(k)
 
-        @pl.when(k < 2)
+        @pl.when(k < half_sp)
         def _():
             near_pair(k, ocore).wait_recv()
 
-        @pl.when(k >= 2)
+        @pl.when(k >= half_sp)
         def _():
             near_copy(k, ocore).wait_recv()
             relay_copy(k, ocore).wait_recv()
@@ -444,22 +466,19 @@
             wts[h] = score.astype(BF16)
             normed_f[:, h * vd : (h + 1) * vd] = dot(wts[h], val[h], 1, 0)
 
-    def turn_of(n):
-        return jnp.where((n >= 1) & (n <= 4), 1 + lax.rem(n, 4), n)
-
     compute(0)
     local_retention()
 
     def step(n, carry):
         k = turn_of(n)
 
-        @pl.when((n < n_sp) & (k == 1))
-        def _():
-            spot = full.at[peer(1), core]
-            push(spot, spot, ssem.at[1], rsem.at[1], (me, far)).wait_recv()
-            near_pair(1, core).start()
-
-        @pl.when((n < n_sp) & (k > 1))
+        @pl.when((n < n_sp) & (k < half_sp))
+        def _():
+            spot = full.at[peer(k), core]
+            push(spot, spot, ssem.at[k], rsem.at[k], (me, far)).wait_recv()
+            near_pair(k, core).start()
+
+        @pl.when((n < n_sp) & (k >= half_sp))
         def _():
             spot = full.at[peer(k), core, plane]
             push(spot, spot, ssem.at[k], rsem.at[k], (me, far)).wait_recv()
@@ -468,7 +487,7 @@
 
         j = turn_of(n - 1)
 
-        @pl.when((n <= n_sp) & (j > 1))
+        @pl.when((n <= n_sp) & (j >= half_sp))
         def _():
             far_copy(j, oplane).wait_recv()
             relay_copy(j, core).start()
@@ -479,7 +498,7 @@
 
         @pl.when(n == pace)
         def _():
-            lax.fori_loop(early, n_sp, send_out, 0)
+            lax.fori_loop(early, n_sp, send_rest, 0)
 
         @pl.when(n == 1)
         def _():
@@ -684,15 +703,15 @@
         part_copy(k).wait_send()
         x_copy(k).wait_send()
 
-        @pl.when(k < 2)
+        @pl.when(k < half_sp)
         def _():
             near_pair(k, core).wait_send()
 
-        @pl.when(k == 1)
-        def _():
-            out_pair().wait_send()
-
-        @pl.when(k >= 2)
+        @pl.when((k > 0) & (k < half_sp))
+        def _():
+            out_pair(k).wait_send()
+
+        @pl.when(k >= half_sp)
         def _():
             out_copy(k).wait_send()
             far_copy(k, plane).wait_send()
@@ -759,13 +778,13 @@
     outs = pl.pallas_call(
         functools.partial(whole_kernel, n_sp, n_tp, heads),
         out_shape=(
-            jax.ShapeDtypeStruct(gate_weight.shape, BF16),
-            jax.ShapeDtypeStruct(up_weight.shape, BF16),
-            jax.ShapeDtypeStruct(down_weight.shape, BF16),
-            jax.ShapeDtypeStruct((w, heads * vd), F32),
-            jax.ShapeDtypeStruct((tokens, heads * kd), BF16),
-            jax.ShapeDtypeStruct((tokens, heads * kd), BF16),
-            jax.ShapeDtypeStruct((tokens, heads * vd), BF16),
+            vmem(gate_weight.shape, BF16),
+            vmem(up_weight.shape, BF16),
+            vmem(down_weight.shape, BF16),
+            vmem((w, heads * vd), F32),
+            vmem((tokens, heads * kd), BF16),
+            vmem((tokens, heads * kd), BF16),
+            vmem((tokens, heads * vd), BF16),
         ),
         in_specs=vmem_specs(12) + [pl.BlockSpec(memory_space=pltpu.HBM)] * 4,
         out_specs=tuple(vmem_specs(7)),
@@ -814,7 +833,7 @@
         + [dma((count,))] * 8
         + [dma((2, n_sp // 2))] * 4,
         compiler_params=pltpu.CompilerParams(
-            collective_id=0, has_side_effects=True, vmem_limit_bytes=48 * 2**20
+            collective_id=0, has_side_effects=True, vmem_limit_bytes=58 * 2**20
         ),
         name="whole",
     )(

time: 98.8 us -> 87.4 us (0.88)
  local copies, waits for them, and re-layouts: 9.74 us -> 0 us
  Pallas kernels: 87.9 us -> 86.6 us
    unnamed x24 -> x0, local copies, waits for them, and re-layouts: 9.74 us -> none
    pallas_call x1, Pallas kernels: 85.3 us -> 84 us  [per_device(): pl.pallas_call(functools.partial(whole_kernel, n_sp, n_tp, heads), out_sh...]
where the time goes in v4:
time: 87.4 us; the launch traced here: 87.2 us
  Pallas kernels  86.6 us (99%)
    pallas_call x1, Pallas kernels, per_device(): pl.pallas_call(functools.partial(whole_kernel, n_sp, n_tp, heads), out_sh...  84 us
    pallas_call x1, Pallas kernels, per_device(): pl.pallas_call(finish_kernel, out_shape=tuple(shapes), in_specs=vmem_spec...  2.56 us

profile of v4, /device:TPU:0, one launch (start us, length us, event | category | flops | bytes accessed | tf_op | source)
XLA Modules:
  0.0 87.2 jit_solution(4675081625399556470)
XLA Ops:
  0.6 84.0 %whole.1 = (bf16[1,2048,256]{2,1,0:T(8,128)(2,1)S(1)}, bf16[1,2048,256]{2,1,0:T(8,128)(2,1)S(1)}, bf16[1,256,2048]{2,1,0:T(8,128)(2,1)S(1)}, f32[256,512]{1,0:T(...) custom-call(bf16[128,2048]{1,0:T(8,128)(2,1)} %stream.1, ...), custom_call_target="tpu_custom_call" | custom-call | tf_op jit(solution)/shard_map/whole/pallas_call | solution.py:778
  84.7 2.6 %finish.1 = (bf16[1,2048,256]{2,1,0:T(8,128)(2,1)}, bf16[1,2048,256]{2,1,0:T(8,128)(2,1)}, bf16[1,256,2048]{2,1,0:T(8,128)(2,1)}, f32[256,512]{1,0:T(8,128)}, bf...) custom-call(bf16[1,2048,256]{2,1,0:T(8,128)(2,1)S(1)} %get-tuple-element.14.gate, ...), custom_call_target="tpu_custom_call" | custom-call | tf_op jit(solution)/shard_map/finish/pallas_call | solution.py:846

commit v5 on v4

--- a/solution.py
+++ b/solution.py
@@ -189,6 +189,13 @@
     return lax.dot_general(a, b, (((da,), (db,)), ((), ())), preferred_element_type=F32)
 
 
+def fine(a, b, da, db):
+    return lax.dot_general(
+        a.astype(F32), b.astype(F32), (((da,), (db,)), ((), ())), preferred_element_type=F32,
+        precision=lax.Precision.HIGHEST,
+    )
+
+
 def flat(block):
     n, cap, q = block.shape
     if cap % 16 == 0:
@@ -209,10 +216,10 @@
     gate_o, up_o, down_o, proj_o, query_o, key_o, value_o,
     full, pack, gu, dw, pw, act, gug, back, part, xbuf, xrecv, sendbuf, ret,
     pick, wcol, slotmap, weight_map, resid, rcols, normed_own, normed_all, normed_f, inv, dec, rem_,
-    mask, wts, qr, kr, val, cosb, sinb, totb, toto, inner, inner_g, incoming, proj,
+    mask, wts, qr, kr, qrf, krf, grad_f, val, cosb, sinb, totb, toto, inner, inner_g, incoming, proj,
     fzin, fzout, fmin, fmout, bzin, bzout, bmin, bmout,
     wsem, tsem, ssem, rsem, fs, fr, ns, nr, es, er, ps, pr, xs, xr, hs, hr, gs, gr,
-    cs, cr, ds, dr, *more,
+    cs, cr, ds, dr, as_, ar, bs, br, *more,
 ):
     fsem, bsem, chain_sem = more[0:4], more[4:8], more[8:12]
     me = lax.axis_index("sp")
@@ -221,6 +228,7 @@
     ocore, oplane = 1 - core, 1 - plane
     far = lax.rem(c + n_tp // 2, n_tp)
     near = c + 1 - 2 * core
+    near_far = lax.rem(near + n_tp // 2, n_tp)
     other = me + 1 - 2 * lax.rem(me, 2)
     cap, q = full.shape[4:]
     hid = dw.shape[0]
@@ -353,9 +361,11 @@
     rows_of = kd // SPLIT
     for h in range(heads):
         x = queries[:, h, :].astype(F32)
-        qr[h] = (x * cosines + swapped(x) * sines).astype(BF16)
+        qrf[h] = x * cosines + swapped(x) * sines
+        qr[h] = qrf[h].astype(BF16)
         x = keys[:, h, :].astype(F32)
         key = (x * cosines + swapped(x) * sines) * scale
+        krf[h] = key
         kr[h] = key.astype(BF16)
         val[h] = values[:, h, :]
         along = jnp.broadcast_to(running[h : h + 1, :], (tokens, tokens))
@@ -462,9 +472,9 @@
 
     def local_retention():
         for h in range(heads):
-            score = dot(qr[h], kr[h], 1, 1) * mask[h]
+            score = fine(qrf[h], krf[h], 1, 1) * mask[h]
             wts[h] = score.astype(BF16)
-            normed_f[:, h * vd : (h + 1) * vd] = dot(wts[h], val[h], 1, 0)
+            normed_f[:, h * vd : (h + 1) * vd] = fine(score, val[h], 1, 0)
 
     compute(0)
     local_retention()
@@ -528,7 +538,7 @@
         incoming[j // SPLIT, pl.ds((j % SPLIT) * rows_of, rows_of), :] = past.result(j)
     for h in range(heads):
         band = slice(h * vd, (h + 1) * vd)
-        kept = normed_f[:, band] + dec[h] * dot(qr[h], incoming[h], 1, 0)
+        kept = normed_f[:, band] + dec[h] * fine(qrf[h], incoming[h], 1, 0)
         inverse = lax.rsqrt(jnp.mean(kept * kept, axis=1, keepdims=True) + EPSILON)
         inv[h] = inverse
         normed_f[:, band] = kept * inverse
@@ -558,7 +568,6 @@
         sent.append(push(mine, mine, gs.at[1, i], gr.at[1, i], (me, near)))
     for cp in sent:
         cp.start()
-    spread.step(1)
 
     def share(side, p):
         return dot(resid[side, p], pw[cols(2 * p + side), :], 1, 0)
@@ -570,6 +579,7 @@
         onward = push(spot, spot, gs.at[2, i], gr.at[2, i], (me, near))
         onward.start()
         sent.append(onward)
+    spread.step(1)
     normed_grad = normed_grad + share(core, oplane)
     for j, p in ((1, plane), (2, oplane)):
         for i in range(2):
@@ -581,23 +591,53 @@
     per_quarter = q // group
     per_group = group * n_sp // (q * n_tp)
 
-    def band_of(index):
+    strips = tokens // n_tp
+
+    def band_of(index, strip_of):
         g = index // per_group
         quarter = g // per_quarter
         return resid.at[
-            lax.rem(quarter, 2), quarter // 2, pl.ds(core * half, half),
+            lax.rem(quarter, 2), quarter // 2,
+            pl.ds(pl.multiple_of(strip_of * strips, 16), strips),
             pl.ds(pl.multiple_of(lax.rem(g, per_quarter) * group, 128), group),
         ]
 
     def col_copy(k):
-        return push(band_of(peer(k)), rcols.at[me, core], cs.at[k], cr.at[k], (peer(k), c))
-
-    def col_near(k, side):
-        spot = rcols.at[peer(k), side]
+        return push(
+            band_of(peer(k), c), rcols.at[me, c], cs.at[k], cr.at[k], (peer(k), c)
+        )
+
+    def col_far(k, t):
+        spot = rcols.at[peer(k), t]
+        return push(spot, spot, as_.at[k], ar.at[k], (me, far))
+
+    def col_near(k, t):
+        spot = rcols.at[peer(k), t]
         return push(spot, spot, ds.at[k], dr.at[k], (me, near))
+
+    def col_relay(k, t):
+        spot = rcols.at[peer(k), t]
+        return push(spot, spot, bs.at[k], br.at[k], (me, near))
 
     def send_cols(k, carry):
         col_copy(k).start()
+        return carry
+
+    def share_cols(k, carry):
+        spot = rcols.at[peer(k), c]
+        push(spot, spot, cs.at[k], cr.at[k], (me, far)).wait_recv()
+        col_far(k, c).start()
+        col_near(k, c).start()
+        return carry
+
+    def relay_cols(k, carry):
+        col_far(k, far).wait_recv()
+        col_relay(k, far).start()
+        return carry
+
+    def wait_cols(k, carry):
+        col_near(k, near).wait_recv()
+        col_relay(k, near_far).wait_recv()
         return carry
 
     grads = []
@@ -606,9 +646,10 @@
         ng = normed_grad[:, band]
         nf = normed_f[:, band]
         grad = inv[h] * (ng - nf * jnp.mean(ng * nf, axis=1, keepdims=True))
+        grad_f[h] = grad
         grad_bf = grad.astype(BF16)
         grads.append(grad_bf)
-        turned = (qr[h].astype(F32) * dec[h]).astype(BF16)
+        turned = (qrf[h] * dec[h]).astype(BF16)
         state = dot(turned, grad_bf, 0, 0)
         for s in range(SPLIT):
             inner_g[h * SPLIT + s] = state[s * rows_of : (s + 1) * rows_of]
@@ -626,58 +667,49 @@
         coming.step(inner_g)
 
     lax.fori_loop(1, n_sp, send_cols, 0)
+    for t in range(n_tp):
+        rcols[me, t] = band_of(me, t)[...]
+    last = max(pairs, n_tp) - 1
 
     def late(s, carry):
+        for d in range(2, pairs):
+
+            @pl.when(s == d - 1)
+            def _():
+                spread.step(d)
+
+        @pl.when(s == last)
+        def _():
+            lax.fori_loop(1, n_sp, share_cols, 0)
+
+        @pl.when((s > 0) & (s < n_tp))
+        def _():
+            weights_grad(s)
+
+        @pl.when(s == last)
+        def _():
+            lax.fori_loop(1, n_sp, relay_cols, 0)
+
         @pl.when((s == coming.slot) & (s > 0))
         def _():
             coming.step(inner_g)
 
-        if pairs > 2:
-
-            @pl.when(s == 1)
-            def _():
-                spread.step(2)
-
-        @pl.when(s < n_tp)
-        def _():
-            weights_grad(s)
-
         return carry
 
-    lax.fori_loop(0, max(pairs, n_tp), late, 0)
-    for d in range(3, pairs):
-        spread.step(d)
-    for side in range(2):
-        g = me // per_group
-        quarter = g // per_quarter
-        rcols[me, side] = resid[
-            lax.rem(quarter, 2), quarter // 2, side * half : (side + 1) * half,
-            pl.ds(pl.multiple_of(lax.rem(g, per_quarter) * group, 128), group),
-        ]
-
-    def relay_cols(k, carry):
-        spot = rcols.at[peer(k), core]
-        push(spot, spot, cs.at[k], cr.at[k], (me, far)).wait_recv()
-        col_near(k, core).start()
-        return carry
-
-    lax.fori_loop(1, n_sp, relay_cols, 0)
+    lax.fori_loop(1, last + 1, late, 0)
+    weights_grad(0)
 
     def unturn(x):
         return x * cosb[...] - swapped(x) * sinb[...]
 
     partial = []
     for h in range(heads):
-        score = (dot(grads[h], val[h], 1, 1) * mask[h]).astype(BF16)
-        qp = dot(score, kr[h], 1, 0) + dec[h] * dot(grads[h], incoming[h], 1, 1)
+        score = (fine(grad_f[h], val[h], 1, 1) * mask[h]).astype(BF16)
+        qp = dot(score, kr[h], 1, 0) + dec[h] * fine(grad_f[h], incoming[h], 1, 1)
         query_o[:, h * kd : (h + 1) * kd] = unturn(qp).astype(BF16)
         partial.append((dot(score, qr[h], 0, 0), dot(wts[h], grads[h], 0, 0)))
 
-    def near_cols(k, carry):
-        col_near(k, ocore).wait_recv()
-        return carry
-
-    lax.fori_loop(1, n_sp, near_cols, 0)
+    lax.fori_loop(1, n_sp, wait_cols, 0)
     spread.finish()
     columns = rcols[...].reshape(n_sp * tokens, group)
     everyone = normed_all[...].reshape(n_sp * tokens, heads * vd)
@@ -722,7 +754,9 @@
         def _():
             home_copy(k).wait_send()
             col_copy(k).wait_send()
-            col_near(k, core).wait_send()
+            col_far(k, c).wait_send()
+            col_near(k, c).wait_send()
+            col_relay(k, far).wait_send()
 
         return carry
 
@@ -804,7 +838,7 @@
             vmem((n_sp, tokens), F32),
             vmem((n_sp, tokens), F32),
             vmem((2, 2, tokens, q), BF16),
-            vmem((n_sp, 2, tokens // 2, group), BF16),
+            vmem((n_sp, n_tp, tokens // n_tp, group), BF16),
             vmem((tokens, heads * vd), BF16),
             vmem((n_sp, tokens, heads * vd), BF16),
             vmem((tokens, heads * vd), F32),
@@ -815,6 +849,9 @@
             vmem((heads, tokens, tokens), BF16),
             vmem((heads, tokens, kd), BF16),
             vmem((heads, tokens, kd), BF16),
+            vmem((heads, tokens, kd), F32),
+            vmem((heads, tokens, kd), F32),
+            vmem((heads, tokens, vd), F32),
             vmem((heads, tokens, vd), BF16),
             vmem((tokens, kd), F32),
             vmem((tokens, kd), F32),
@@ -829,7 +866,7 @@
         + [dma((4,)), dma((2,))]
         + [dma((n_sp,))] * 14
         + [dma((3, 2))] * 2
-        + [dma((n_sp,))] * 4
+        + [dma((n_sp,))] * 8
         + [dma((count,))] * 8
         + [dma((2, n_sp // 2))] * 4,
         compiler_params=pltpu.CompilerParams(

time: 87.4 us -> 83.3 us (0.953)
  Pallas kernels: 86.6 us -> 82.5 us
    pallas_call x1, Pallas kernels: 84 us -> 80 us  [per_device(): pl.pallas_call(functools.partial(whole_kernel, n_sp, n_tp, heads), out_sh...]
where the time goes in v5:
time: 83.3 us; the launch traced here: 83.2 us
  Pallas kernels  82.5 us (99%)
    pallas_call x1, Pallas kernels, per_device(): pl.pallas_call(functools.partial(whole_kernel, n_sp, n_tp, heads), out_sh...  80 us
    pallas_call x1, Pallas kernels, per_device(): pl.pallas_call(finish_kernel, out_shape=tuple(shapes), in_specs=vmem_spec...  2.56 us

profile of v5, /device:TPU:0, one launch (start us, length us, event | category | flops | bytes accessed | tf_op | source)
XLA Modules:
  0.0 83.2 jit_solution(2117015632109735937)
XLA Ops:
  0.6 80.0 %whole.1 = (bf16[1,2048,256]{2,1,0:T(8,128)(2,1)S(1)}, bf16[1,2048,256]{2,1,0:T(8,128)(2,1)S(1)}, bf16[1,256,2048]{2,1,0:T(8,128)(2,1)S(1)}, f32[256,512]{1,0:T(...) custom-call(bf16[128,2048]{1,0:T(8,128)(2,1)} %stream.1, ...), custom_call_target="tpu_custom_call" | custom-call | tf_op jit(solution)/shard_map/whole/pallas_call | solution.py:812
  80.6 2.6 %finish.1 = (bf16[1,2048,256]{2,1,0:T(8,128)(2,1)}, bf16[1,2048,256]{2,1,0:T(8,128)(2,1)}, bf16[1,256,2048]{2,1,0:T(8,128)(2,1)}, f32[256,512]{1,0:T(8,128)}, bf...) custom-call(bf16[1,2048,256]{2,1,0:T(8,128)(2,1)S(1)} %get-tuple-element.14.gate, ...), custom_call_target="tpu_custom_call" | custom-call | tf_op jit(solution)/shard_map/finish/pallas_call | solution.py:883
